TPU v7x, 32 devices: a whole 2x2x4 slice. The times are simulated.
32 devices in a mesh: dp: 4 (over y, x), kv: 4 (over z), tp: 2 (over core).
Axes of the slice: x: 2, y: 2, z: 4, core: 2. Of those that a mesh axis runs over, the one named last changes fastest.
Arguments:
- resid: bfloat16 [16, 2048], P('dp', ('kv', 'tp')), may hold values from -45 to 45
- norm_gain: bfloat16 [3, 2048], P(None, ('kv', 'tp')), may hold values from 0.099609375 to 1.8984375
- ffn_gate: bfloat16 [2, 2048, 5632], P(None, None, ('kv', 'tp')), may hold values from -0.125 to 0.125
- ffn_up: bfloat16 [2, 2048, 5632], P(None, None, ('kv', 'tp')), may hold values from -0.125 to 0.125
- ffn_down: bfloat16 [2, 5632, 2048], P(None, ('kv', 'tp')), may hold values from -0.109375 to 0.109375
- w_x: bfloat16 [2048, 64, 64], P(None, 'kv', 'tp'), may hold values from -0.125 to 0.125
- w_z: bfloat16 [2048, 64, 64], P(None, 'kv', 'tp'), may hold values from -0.125 to 0.125
- w_bc: bfloat16 [2048, 2, 8, 128], P('kv'), may hold values from -0.125 to 0.125
- w_dt: bfloat16 [2048, 64], P('kv'), may hold values from -0.125 to 0.125
- dt_bias: float32 [64], replicated, may hold values from -2 to 0.5
- a_log: float32 [64], replicated, may hold values from -1.5 to 1.5
- d_skip: float32 [64], replicated, may hold values from 0.5 to 1.5
- conv_wx: bfloat16 [4, 64, 64], P(None, None, 'tp'), may hold values from -3 to 3
- conv_wbc: bfloat16 [4, 2, 8, 128], replicated, may hold values from -3 to 3
- conv_x: bfloat16 [16, 3, 64, 64], P(('dp', 'kv'), None, None, 'tp'), may hold values from -6 to 6
- conv_bc: bfloat16 [16, 3, 2, 8, 128], P(('dp', 'kv')), may hold values from -6 to 6
- ssm_state: float32 [16, 64, 64, 128], P(('dp', 'kv'), None, 'tp'), may hold values from -3 to 3
- w_out: bfloat16 [64, 64, 2048], P(None, 'tp', 'kv'), may hold values from -0.09375 to 0.09375
Outputs:
- final: bfloat16 [16, 2048], P('dp', ('kv', 'tp'))
All inputs are finite; a program needn't handle non-finite values.
Results may differ from a plain program's by a relative error of at most 0.018.
Values may be sent and summed in bfloat16 or wider, within the bound.
A program may use at most 64 MiB of HBM per device.

v0:
```python
import functools

import jax
import jax.numpy as jnp
from jax import lax
from jax.experimental import pallas as pl
from jax.experimental.pallas import tpu as pltpu
from jax.sharding import PartitionSpec as P

D = 2048
F32 = jnp.float32
BF16 = jnp.bfloat16
MESH = pl.DeviceIdType.MESH

EPS = 1e-06


def normalize(rows, gain):
    values = rows.astype(jnp.float32)
    scale = lax.rsqrt(jnp.mean(values * values, axis=1, keepdims=True) + EPS)
    return (values * scale * gain.astype(jnp.float32).reshape(1, -1)).astype(jnp.bfloat16)


def feed_forward(normed, w_gate, w_up, w_down):
    gate = jnp.dot(normed, w_gate, preferred_element_type=jnp.float32)
    upper = jnp.dot(normed, w_up, preferred_element_type=jnp.float32)
    hidden = (jax.nn.silu(gate) * upper).astype(jnp.bfloat16)
    return jnp.dot(hidden, w_down, preferred_element_type=jnp.float32)


def add_half(base, sums):
    return (base.astype(jnp.float32) + 0.5 * sums).astype(jnp.bfloat16)


def ffn_totals(partial_value):
    return lax.psum(partial_value, ("kv", "tp"))


def short_conv(history, newest, taps):
    window = jnp.concatenate(
        [history.astype(jnp.float32), newest.astype(jnp.float32)[:, None]], axis=1
    )
    return jax.nn.silu(jnp.sum(window * taps.astype(jnp.float32)[None], axis=1))


def state_step(
    xs_new,
    zeta,
    bc_new,
    dt_raw,
    conv_x,
    conv_bc,
    ssm_state,
    conv_wx,
    conv_wbc,
    dt_bias,
    a_log,
    d_skip,
):
    xconv = short_conv(conv_x, xs_new, conv_wx)
    bconv = short_conv(conv_bc, bc_new, conv_wbc)
    heads = xconv.shape[1]
    groups = bconv.shape[2]
    bmat = jnp.repeat(bconv[:, 0], heads // groups, axis=1)
    cmat = jnp.repeat(bconv[:, 1], heads // groups, axis=1)
    step_size = jax.nn.softplus(dt_raw + dt_bias[None, :])
    decay = jnp.exp(-step_size * jnp.exp(a_log)[None, :])
    updated = (
        decay[:, :, None, None] * ssm_state
        + (step_size[:, :, None] * xconv)[..., None] * bmat[:, :, None, :]
    )
    mixed = (
        jnp.einsum("shpn,shn->shp", updated, cmat, precision=lax.Precision.HIGHEST)
        + d_skip[None, :, None] * xconv
    )
    return (mixed * jax.nn.silu(zeta.astype(jnp.float32))).astype(jnp.bfloat16)


def group_terms(slab, w_bc, w_dt):
    span = slab.shape[1]
    flat_bc = w_bc.reshape(span, -1)
    bc_part = jnp.dot(slab, flat_bc, preferred_element_type=jnp.float32)
    dt_part = jnp.dot(slab, w_dt, preferred_element_type=jnp.float32)
    return (
        lax.psum_scatter(bc_part, "kv", scatter_dimension=0, tiled=True),
        lax.psum_scatter(dt_part, "kv", scatter_dimension=0, tiled=True),
    )


def mix_partial(
    normed,
    w_x,
    w_z,
    w_bc,
    w_dt,
    dt_bias,
    a_log,
    d_skip,
    conv_wx,
    conv_wbc,
    conv_x,
    conv_bc,
    ssm_state,
    w_out,
):
    rows = normed.shape[0]
    local_heads = w_x.shape[1]
    half = w_x.shape[2]
    xs_part = (
        jnp.dot(normed, w_x.reshape(D, -1), preferred_element_type=jnp.float32)
        .astype(jnp.bfloat16)
        .reshape(rows, local_heads, half)
    )
    zeta_part = (
        jnp.dot(normed, w_z.reshape(D, -1), preferred_element_type=jnp.float32)
        .astype(jnp.bfloat16)
        .reshape(rows, local_heads, half)
    )
    xs_new, zeta = (
        lax.all_to_all(xs_part, "kv", split_axis=0, concat_axis=1, tiled=True),
        lax.all_to_all(zeta_part, "kv", split_axis=0, concat_axis=1, tiled=True),
    )
    span = w_bc.shape[0]
    slab = lax.dynamic_slice_in_dim(normed, lax.axis_index("kv") * span, span, 1)
    bc_sum, dt_raw = group_terms(slab, w_bc, w_dt)
    bc_new = bc_sum.astype(jnp.bfloat16).reshape((bc_sum.shape[0],) + w_bc.shape[1:])
    mixed = state_step(
        xs_new,
        zeta,
        bc_new,
        dt_raw,
        conv_x,
        conv_bc,
        ssm_state,
        conv_wx,
        conv_wbc,
        dt_bias,
        a_log,
        d_skip,
    )
    flat_out = w_out.reshape(-1, w_out.shape[2])
    piece = lax.all_gather(mixed, "kv", axis=0, tiled=True)
    return jnp.dot(piece.reshape(piece.shape[0], -1), flat_out, preferred_element_type=jnp.float32)


def per_device(
    resid,
    norm_gain,
    ffn_gate,
    ffn_up,
    ffn_down,
    w_x,
    w_z,
    w_bc,
    w_dt,
    dt_bias,
    a_log,
    d_skip,
    conv_wx,
    conv_wbc,
    conv_x,
    conv_bc,
    ssm_state,
    w_out,
):
    mixer_args = (
        w_x,
        w_z,
        w_bc,
        w_dt,
        dt_bias,
        a_log,
        d_skip,
        conv_wx,
        conv_wbc,
        conv_x,
        conv_bc,
        ssm_state,
        w_out,
    )
    rows, gains = (
        lax.all_gather(resid, ("kv", "tp"), axis=1, tiled=True),
        lax.all_gather(norm_gain, ("kv", "tp"), axis=1, tiled=True),
    )
    first = add_half(
        rows,
        ffn_totals(feed_forward(normalize(rows, gains[0]), ffn_gate[0], ffn_up[0], ffn_down[0])),
    )
    partial_value = mix_partial(normalize(first, gains[1]), *mixer_args)
    span = partial_value.shape[1]
    block = lax.dynamic_slice_in_dim(first, lax.axis_index("kv") * span, span, 1)
    joined = (block.astype(jnp.float32) + lax.psum(partial_value, "tp")).astype(jnp.bfloat16)
    second = lax.all_gather(joined, "kv", axis=1, tiled=True)
    final = add_half(
        second,
        ffn_totals(feed_forward(normalize(second, gains[2]), ffn_gate[1], ffn_up[1], ffn_down[1])),
    )
    width = resid.shape[1]
    return lax.dynamic_slice_in_dim(final, lax.axis_index(("kv", "tp")) * width, width, 1)


def nt_dot(left, right):
    return lax.dot_general(left, right, (((1,), (1,)), ((), ())), preferred_element_type=F32)


def nn_dot(left, right):
    return jnp.dot(left, right, preferred_element_type=F32)


def silu(value):
    return value * jax.nn.sigmoid(value)


def norm_rows(values, gain):
    scale = lax.rsqrt(jnp.mean(values * values, axis=1, keepdims=True) + EPS)
    return (values * scale * gain).astype(BF16)


def split_two(value):
    high = value.astype(BF16)
    return high, (value - high.astype(F32)).astype(BF16)


def layer_kernel(
    nk,
    nt,
    resid,
    gains,
    gate,
    up,
    down,
    wx,
    wz,
    wbc,
    wdt,
    dt_bias,
    a_log,
    d_skip,
    cwx,
    cwbc,
    cx,
    cbc,
    state,
    wout,
    out,
    gate_v,
    up_v,
    down_v,
    wx_v,
    wz_v,
    wbc_v,
    wdt_v,
    state_v,
    wout_v,
    state_b,
    small_v,
    cwx_v,
    cwbc_v,
    cx_v,
    cbc_v,
    expand_v,
    repeat_v,
    xn_v,
    rows_s,
    gain_s,
    first_v,
    part_b,
    near_s,
    half_s,
    xz_b,
    bc_b,
    dt_b,
    xz_s,
    bc_s,
    dt_s,
    mix_s,
    proj_s,
    second_v,
    cut_b,
    cut_s,
    load_sem,
    rows_send,
    rows_recv,
    gain_send,
    gain_recv,
    near_send,
    near_recv,
    half_send,
    half_recv,
    xz_send,
    xz_recv,
    bc_send,
    bc_recv,
    dt_send,
    dt_recv,
    mix_send,
    mix_recv,
    proj_send,
    proj_recv,
    cut_send,
    cut_recv,
):
    me_k, me_t = lax.axis_index("kv"), lax.axis_index("tp")
    n = nk * nt
    me = me_k * nt + me_t
    rows, width = rows_s.shape[1], rows_s.shape[2]
    dim = n * width

    def target(index):
        return {"kv": lax.div(index, nt), "tp": lax.rem(index, nt)}

    def flipped(index, mask):
        bit = 1
        while bit < nk:
            if mask & bit:
                index = index + bit - 2 * bit * lax.rem(lax.div(index, bit), 2)
            bit *= 2
        return index

    def all_peers():
        order = [(x, d) for x in range(nk) for d in range(nt)][1:]
        return [flipped(me_k, x) * nt + lax.rem(me_t + d, nt) for x, d in order]

    def kv_peers():
        return [flipped(me_k, x) for x in range(1, nk)]

    loads = {}

    def load(name, src, dst):
        copy = pltpu.make_async_copy(src, dst, load_sem.at[len(loads)])
        copy.start()
        loads[name] = copy

    load("rows", resid, rows_s.at[me])
    load("gains", gains, gain_s.at[me])
    load("gate0", gate.at[0], gate_v.at[0])
    load("up0", up.at[0], up_v.at[0])
    load("down0", down.at[0], down_v.at[0])
    load("bias", dt_bias, small_v.at[0])
    load("alog", a_log, small_v.at[1])
    load("skip", d_skip, small_v.at[2])
    load("cwx", cwx, cwx_v)
    load("cwbc", cwbc, cwbc_v)
    load("cx", cx, cx_v)
    load("cbc", cbc, cbc_v)
    load("wx", wx, wx_v)
    load("wz", wz, wz_v)
    load("wbc", wbc, wbc_v)
    load("wdt", wdt, wdt_v)
    load("state", state, state_v)
    load("wout", wout, wout_v)
    load("gate1", gate.at[1], gate_v.at[1])
    load("up1", up.at[1], up_v.at[1])
    load("down1", down.at[1], down_v.at[1])

    barrier = pltpu.get_barrier_semaphore()
    for q in all_peers():
        pl.semaphore_signal(barrier, inc=1, device_id=target(q), device_id_type=MESH)
    pl.semaphore_wait(barrier, n - 1)

    def send(src, dst, ssem, rsem, index):
        copy = pltpu.make_async_remote_copy(
            src_ref=src,
            dst_ref=dst,
            send_sem=ssem,
            recv_sem=rsem,
            device_id=target(index),
            device_id_type=MESH,
        )
        copy.start()
        return copy

    def arrived(slots, ssem, rsem, index):
        pltpu.make_async_remote_copy(
            src_ref=slots.at[index],
            dst_ref=slots.at[index],
            send_sem=ssem.at[index],
            recv_sem=rsem.at[index],
            device_id=target(index),
            device_id_type=MESH,
        ).wait_recv()

    sent = []

    loads["rows"].wait()
    loads["gains"].wait()
    for q in all_peers()[::-1]:
        sent.append(send(rows_s.at[me], rows_s.at[me], rows_send.at[q], rows_recv.at[me], q))
    for q in all_peers()[::-1]:
        sent.append(send(gain_s.at[me], gain_s.at[me], gain_send.at[q], gain_recv.at[me], q))

    heads, half = cx_v.shape[2], cx_v.shape[1]
    flat = heads * half
    groups = cwbc_v.shape[1] // 2
    pairs = 2 * groups
    lane = lax.broadcasted_iota(jnp.int32, expand_v.shape, 1)
    head_of = lax.broadcasted_iota(jnp.int32, expand_v.shape, 0) * half
    expand_v[...] = jnp.where((lane >= head_of) & (lane < head_of + half), 1.0, 0.0).astype(BF16)
    lane = lax.broadcasted_iota(jnp.int32, repeat_v.shape, 1)
    src_of = lax.broadcasted_iota(jnp.int32, repeat_v.shape, 0) * pairs
    repeat_v[...] = jnp.where((lane >= src_of) & (lane < src_of + pairs), 1.0, 0.0).astype(BF16)

    units = gate_v.shape[1]

    def gated(blocks, which):
        squares = jnp.zeros((rows, 1), F32)
        g = jnp.zeros((rows, units), F32)
        u = jnp.zeros((rows, units), F32)
        for values, gain, at in blocks:
            squares = squares + jnp.sum(values * values, axis=1, keepdims=True)
            left = (values * gain).astype(BF16)
            g = g + nt_dot(left, gate_v[which, :, at])
            u = u + nt_dot(left, up_v[which, :, at])
        scale = lax.rsqrt(squares / dim + EPS)
        return (silu(g * scale) * (u * scale)).astype(BF16)

    def columns(index, count):
        return pl.ds(pl.multiple_of(index * count, 128), count)

    def arriving_rows():
        for q in [me] + all_peers():
            if q is not me:
                arrived(rows_s, rows_send, rows_recv, q)
                arrived(gain_s, gain_send, gain_recv, q)
            yield rows_s[q].astype(F32), gain_s[q, 0:1, :].astype(F32), columns(q, width)

    loads["gate0"].wait()
    loads["up0"].wait()
    hidden = gated(arriving_rows(), 0)
    loads["down0"].wait()
    wide = dim // nt
    for d in range(1, nt):
        t = lax.rem(me_t + d, nt)
        part_b[t] = nn_dot(hidden, down_v[0, :, columns(t, wide)]).astype(BF16)
        sent.append(
            send(part_b.at[t], near_s.at[me_t], near_send.at[t], near_recv.at[me_t], me_k * nt + t)
        )

    chip = nn_dot(hidden, down_v[0, :, columns(me_t, wide)])

    def gain_row(i):
        return jnp.concatenate(
            [gain_s[q, i : i + 1, :].astype(F32) for q in range(n)], axis=1
        )

    base = jnp.concatenate([rows_s[q].astype(F32) for q in range(n)], axis=1)

    def two_nt(first_w, second_w):
        one = jnp.zeros((rows, first_w.shape[0]), F32)
        two = jnp.zeros((rows, first_w.shape[0]), F32)
        for k in range(n):
            left = xn_v[:, k * width : (k + 1) * width]
            one = one + nt_dot(left, first_w[:, k * width : (k + 1) * width])
            two = two + nt_dot(left, second_w[:, k * width : (k + 1) * width])
        return one, two

    for d in range(1, nt):
        t = lax.rem(me_t + d, nt)
        pltpu.make_async_remote_copy(
            src_ref=near_s.at[t],
            dst_ref=near_s.at[t],
            send_sem=near_send.at[t],
            recv_sem=near_recv.at[t],
            device_id=target(me_k * nt + t),
            device_id_type=MESH,
        ).wait_recv()
    for d in range(1, nt):
        chip = chip + near_s[lax.rem(me_t + d, nt)].astype(F32)
    half_s[me] = chip.astype(BF16)
    for q in all_peers()[::-1]:
        sent.append(send(half_s.at[me], half_s.at[me], half_send.at[q], half_recv.at[me], q))
    for name in ("bias", "alog", "skip", "cwx", "cwbc", "cx", "cbc"):
        loads[name].wait()

    def expand(value):
        return nn_dot(value, expand_v[...])

    known = sum(cx_v[i].astype(F32) * cwx_v[i].astype(F32) for i in range(cx_v.shape[0]))
    high, low = split_two(known)
    lane = lax.broadcasted_iota(jnp.int32, (half, flat), 1)
    row = lax.broadcasted_iota(jnp.int32, (half, flat), 0)
    own = (lane & (half - 1)) == row
    hist_x = jnp.sum(jnp.where(own, expand(high) + expand(low), 0.0), axis=0, keepdims=True)
    tap_x = jnp.sum(jnp.where(own, expand(cwx_v[cx_v.shape[0]]), 0.0), axis=0, keepdims=True)
    skip_high, skip_low = split_two(small_v[2])
    skip_row = expand(skip_high) + expand(skip_low)
    hist_bc = sum(cbc_v[i].astype(F32) * cwbc_v[i].astype(F32) for i in range(cbc_v.shape[0]))
    tap_bc = cwbc_v[cbc_v.shape[0]].astype(F32)

    loads["state"].wait()
    state_b[...] = state_v[...].astype(BF16)
    for q in all_peers():
        arrived(half_s, half_send, half_recv, q)
    total = jnp.concatenate(
        [sum(half_s[k * nt + t].astype(F32) for k in range(nk)) for t in range(nt)], axis=1
    )
    first = (base + 0.5 * total).astype(BF16).astype(F32)
    xn_v[...] = norm_rows(first, gain_row(1))
    block = nt * width
    for k in range(nk):
        first_v[k] = first[:, k * block : (k + 1) * block]

    span = wdt_v.shape[1]
    loads["wbc"].wait()
    loads["wdt"].wait()
    tile = repeat_v.shape[0]
    spread = repeat_v.shape[1]
    lane = lax.broadcasted_iota(jnp.int32, (rows * pairs, spread), 1)
    row = lax.broadcasted_iota(jnp.int32, (rows * pairs, spread), 0)
    same = (lane & (pairs - 1)) == (row & (pairs - 1))
    slab = xn_v[:, pl.ds(pl.multiple_of(me_k * span, 128), span)]
    bc_part = jnp.zeros((rows * pairs, wbc_v.shape[1]), F32)
    for c in range(span // tile):
        piece = slab[:, c * tile : (c + 1) * tile].astype(F32)
        piece = jnp.concatenate(
            [jnp.broadcast_to(piece[r : r + 1], (pairs, tile)) for r in range(rows)], axis=0
        ).astype(BF16)
        wide_x = jnp.where(same, nn_dot(piece, repeat_v[...]), 0.0).astype(BF16)
        bc_part = bc_part + nn_dot(wide_x, wbc_v[c * spread : (c + 1) * spread, :])
    dt_part = nt_dot(slab, wdt_v[...])
    for r in range(rows):
        bc_b[r] = bc_part[r * pairs : (r + 1) * pairs].astype(BF16)
        dt_b[r] = dt_part[r : r + 1]
    bc_s[me_k] = bc_b[me_k]
    dt_s[me_k] = dt_b[me_k]
    for k in kv_peers()[::-1]:
        q = k * nt + me_t
        sent.append(send(bc_b.at[k], bc_s.at[me_k], bc_send.at[k], bc_recv.at[me_k], q))
        sent.append(send(dt_b.at[k], dt_s.at[me_k], dt_send.at[k], dt_recv.at[me_k], q))

    loads["wx"].wait()
    loads["wz"].wait()
    xs_part, z_part = two_nt(wx_v, wz_v)
    cols = xs_part.shape[1]
    for r in range(rows):
        xz_b[r, :, :cols] = xs_part[r : r + 1].astype(BF16)
        xz_b[r, :, cols:] = z_part[r : r + 1].astype(BF16)
    xz_s[me_k] = xz_b[me_k]
    for k in kv_peers()[::-1]:
        q = k * nt + me_t
        sent.append(send(xz_b.at[k], xz_s.at[me_k], xz_send.at[k], xz_recv.at[me_k], q))

    def arrived_kv(slots, ssem, rsem):
        for k in kv_peers():
            pltpu.make_async_remote_copy(
                src_ref=slots.at[k],
                dst_ref=slots.at[k],
                send_sem=ssem.at[k],
                recv_sem=rsem.at[k],
                device_id=target(k * nt + me_t),
                device_id_type=MESH,
            ).wait_recv()

    arrived_kv(dt_s, dt_send, dt_recv)
    raw = sum(dt_s[k] for k in range(nk)) + small_v[0]
    step = jnp.maximum(raw, 0.0) + jnp.log1p(jnp.exp(-jnp.abs(raw)))
    decay = jnp.exp(-step * jnp.exp(small_v[1]))
    step_high, step_low = split_two(step)
    decay_high, decay_low = split_two(decay)
    decay_row = expand(decay_high) + expand(decay_low)
    step_row = expand(step_high) + expand(step_low)
    arrived_kv(bc_s, bc_send, bc_recv)
    bc_new = sum(bc_s[k].astype(F32) for k in range(nk)).astype(BF16).astype(F32)
    bconv = silu(hist_bc + bc_new * tap_bc)
    bmat, cmat = bconv[:groups], bconv[groups:]
    weight = jnp.sum(bmat * cmat, axis=1, keepdims=True)
    per_group = nt_dot(cmat.astype(BF16), state_b[...])
    lane = lax.broadcasted_iota(jnp.int32, (groups, flat), 1)
    low_end = lax.broadcasted_iota(jnp.int32, (groups, flat), 0) * (flat // groups)
    mine = (lane >= low_end) & (lane < low_end + flat // groups)
    read = jnp.sum(jnp.where(mine, per_group, 0.0), axis=0, keepdims=True)
    cross = jnp.sum(jnp.where(mine, weight, 0.0), axis=0, keepdims=True)
    arrived_kv(xz_s, xz_send, xz_recv)
    xs_row = jnp.concatenate([xz_s[k, :, :cols].astype(F32) for k in range(nk)], axis=1)
    z_row = jnp.concatenate([xz_s[k, :, cols:].astype(F32) for k in range(nk)], axis=1)
    xconv = silu(hist_x + xs_row * tap_x)
    mixed = decay_row * read + (step_row * cross + skip_row) * xconv
    mix_s[me_k] = (mixed * silu(z_row)).astype(BF16)
    for k in kv_peers()[::-1]:
        q = k * nt + me_t
        sent.append(send(mix_s.at[me_k], mix_s.at[me_k], mix_send.at[k], mix_recv.at[me_k], q))
    loads["wout"].wait()
    arrived_kv(mix_s, mix_send, mix_recv)
    mixed = jnp.concatenate([mix_s[k].astype(F32) for k in range(nk)], axis=0).astype(BF16)
    proj_s[me] = nn_dot(mixed, wout_v[...]).astype(BF16)
    for q in all_peers()[::-1]:
        sent.append(send(proj_s.at[me], proj_s.at[me], proj_send.at[q], proj_recv.at[me], q))

    def arriving_blocks():
        for x in range(nk):
            k = flipped(me_k, x)
            for d in range(nt):
                if x or d:
                    q = k * nt + lax.rem(me_t + d, nt)
                    arrived(proj_s, proj_send, proj_recv, q)
            total = sum(proj_s[k * nt + t].astype(F32) for t in range(nt))
            second = (first_v[k] + total).astype(BF16).astype(F32)
            if x == 0:
                for t in range(nt):
                    second_v[t] = second[:, t * width : (t + 1) * width]
            gain = jnp.concatenate(
                [gain_s[k * nt + t, 2:3, :].astype(F32) for t in range(nt)], axis=1
            )
            yield second, gain, columns(k, block)

    loads["gate1"].wait()
    loads["up1"].wait()
    hidden = gated(arriving_blocks(), 1)
    loads["down1"].wait()
    for q in all_peers()[::-1]:
        cut_b[q] = nn_dot(hidden, down_v[1, :, columns(q, width)]).astype(BF16)
        sent.append(send(cut_b.at[q], cut_s.at[me], cut_send.at[q], cut_recv.at[me], q))
    total = nn_dot(hidden, down_v[1, :, columns(me, width)])
    for q in all_peers():
        arrived(cut_s, cut_send, cut_recv, q)
        total = total + cut_s[q].astype(F32)
    out[...] = (second_v[me_t] + 0.5 * total).astype(BF16)
    for copy in sent:
        copy.wait_send()


def fused_layer(
    nk,
    nt,
    resid,
    norm_gain,
    ffn_gate,
    ffn_up,
    ffn_down,
    w_x,
    w_z,
    w_bc,
    w_dt,
    dt_bias,
    a_log,
    d_skip,
    conv_wx,
    conv_wbc,
    conv_x,
    conv_bc,
    ssm_state,
    w_out,
):
    n = nk * nt
    rows, width = resid.shape
    dim = ffn_gate.shape[1]
    units = ffn_gate.shape[2]
    local = w_x.shape[1] * w_x.shape[2]
    heads, half = conv_x.shape[2], conv_x.shape[3]
    flat = heads * half
    span = w_bc.shape[0]
    lanes = w_bc.shape[3]
    pairs = w_bc.shape[1] * w_bc.shape[2]
    out_cols = w_out.shape[2]
    taps = conv_wx.shape[0]
    tile = 128
    args = (
        resid,
        norm_gain,
        jnp.swapaxes(ffn_gate, 1, 2),
        jnp.swapaxes(ffn_up, 1, 2),
        ffn_down,
        jnp.transpose(w_x, (1, 2, 0)).reshape(local, dim),
        jnp.transpose(w_z, (1, 2, 0)).reshape(local, dim),
        w_bc.reshape(span * pairs, lanes),
        w_dt.T,
        dt_bias.reshape(1, heads),
        a_log.reshape(1, heads),
        d_skip.reshape(1, heads),
        jnp.swapaxes(conv_wx, 1, 2),
        conv_wbc.reshape(taps, pairs, lanes),
        jnp.swapaxes(conv_x, 2, 3).reshape(taps - 1, half, heads),
        conv_bc.reshape(taps - 1, pairs, lanes),
        ssm_state.reshape(flat, lanes),
        w_out.reshape(flat, out_cols),
    )
    dma = pltpu.SemaphoreType.DMA
    vmem = pltpu.VMEM
    scratch = [
        vmem((2, units, dim), BF16),
        vmem((2, units, dim), BF16),
        vmem((2, units, dim), BF16),
        vmem((local, dim), BF16),
        vmem((local, dim), BF16),
        vmem((span * pairs, lanes), BF16),
        vmem((heads, span), BF16),
        vmem((flat, lanes), F32),
        vmem((flat, out_cols), BF16),
        vmem((flat, lanes), BF16),
        vmem((3, 1, heads), F32),
        vmem((taps, half, heads), BF16),
        vmem((taps, pairs, lanes), BF16),
        vmem((taps - 1, half, heads), BF16),
        vmem((taps - 1, pairs, lanes), BF16),
        vmem((heads, flat), BF16),
        vmem((tile, tile * pairs), BF16),
        vmem((rows, dim), BF16),
        vmem((n, rows, width), BF16),
        vmem((n, 3, width), BF16),
        vmem((nk, rows, dim // nk), F32),
        vmem((nt, rows, dim // nt), BF16),
        vmem((nt, rows, dim // nt), BF16),
        vmem((n, rows, dim // nt), BF16),
        vmem((nk, 1, 2 * local), BF16),
        vmem((nk, pairs, lanes), BF16),
        vmem((nk, 1, heads), F32),
        vmem((nk, 1, 2 * local), BF16),
        vmem((nk, pairs, lanes), BF16),
        vmem((nk, 1, heads), F32),
        vmem((nk, 1, flat), BF16),
        vmem((n, rows, out_cols), BF16),
        vmem((nt, rows, width), F32),
        vmem((n, rows, width), BF16),
        vmem((n, rows, width), BF16),
        dma((21,)),
    ]
    for count in (n, n, nt, n, nk, nk, nk, nk, n, n):
        scratch += [dma((count,)), dma((count,))]
    return pl.pallas_call(
        functools.partial(layer_kernel, nk, nt),
        out_shape=jax.ShapeDtypeStruct(resid.shape, resid.dtype),
        in_specs=[pl.BlockSpec(memory_space=pl.ANY)] * len(args),
        out_specs=pl.BlockSpec(memory_space=pltpu.VMEM),
        scratch_shapes=scratch,
        compiler_params=pltpu.CompilerParams(
            collective_id=0, has_side_effects=True, vmem_limit_bytes=60 * 1024 * 1024
        ),
    )(*args)


def fits(nk, nt, resid, w_x, w_bc, conv_x):
    rows, width = resid.shape
    half = conv_x.shape[3]
    pairs = w_bc.shape[1] * w_bc.shape[2]
    return (
        conv_x.shape[0] == 1
        and rows == nk
        and nt > 1
        and nk & (nk - 1) == 0
        and w_bc.shape[0] == nt * width
        and width % 128 == 0
        and w_bc.shape[0] % 128 == 0
        and (w_x.shape[1] * w_x.shape[2]) % 128 == 0
        and half & (half - 1) == 0
        and pairs & (pairs - 1) == 0
    )


def solution(mesh):
    placed = (
        P("dp", ("kv", "tp")),
        P(None, ("kv", "tp")),
        P(None, None, ("kv", "tp")),
        P(None, None, ("kv", "tp")),
        P(None, ("kv", "tp"), None),
        P(None, "kv", "tp"),
        P(None, "kv", "tp"),
        P("kv", None, None, None),
        P("kv", None),
        P(),
        P(),
        P(),
        P(None, None, "tp"),
        P(),
        P(("dp", "kv"), None, None, "tp"),
        P(("dp", "kv"), None, None, None, None),
        P(("dp", "kv"), None, "tp", None),
        P(None, "tp", "kv"),
    )
    nk, nt = mesh.shape["kv"], mesh.shape["tp"]

    def layer(*args):
        if fits(nk, nt, args[0], args[5], args[7], args[14]):
            return fused_layer(nk, nt, *args)
        return per_device(*args)

    return jax.shard_map(
        layer, mesh=mesh, in_specs=placed, out_specs=P("dp", ("kv", "tp")), check_vma=False
    )
```

profile of v0, /device:TPU:0, one launch (start us, length us, event | category | flops | bytes accessed | tf_op | source)
XLA Modules:
  0.0 36.4 jit_solution(923635467505231608)
XLA Ops:
  0.0 35.1 %shard_map.172 = bf16[4,256]{1,0:T(4,128)(2,1)} custom-call(bf16[4,256]{1,0:T(4,128)(2,1)} %resid.1, bf16[3,256]{1,0:T(4,128)(2,1)} %gains.1, bf16[2,704,2048]{2,1,0:T(8,128)(2,1)} %bitcast.21, bf16[2,704,2048]{2,1,0:T(8,128)(2,1)} %bitcast.22, bf16[2,704,2048]{2,1,0:T(8,128)(2,1)} %down.1, bf16[512,2048]{1,0:T(8,128)(2,1)} %bitcast.23, ...), custom_call_target="tpu_custom_call" | custom-call | tf_op jit(solution)/shard_map/pallas_call | solution.py:719
  35.1 1.3 %copy.20 = bf16[4,256]{1,0:T(4,128)(2,1)} copy(bf16[4,256]{1,0:T(4,128)(2,1)} %shard_map.172) | data formatting | bytes 4096
where the time goes:
time: 36.5 us; the launch traced here: 36.4 us
  Pallas kernels  35.1 us (96%)
  local copies, waits for them, and re-layouts  1.26 us (3%)
    pallas_call x1, Pallas kernels, fused_layer(): pl.pallas_call(functools.partial(layer_kernel, nk, nt), out_shape=jax.Sha...  35.1 us
    unnamed x1, local copies, waits for them, and re-layouts  1.26 us

commit v1 on v0

--- a/solution.py
+++ b/solution.py
@@ -712,13 +712,17 @@
         vmem((nt, rows, width), F32),
         vmem((n, rows, width), BF16),
         vmem((n, rows, width), BF16),
-        dma((21,)),
     ]
+    sems = [dma((21,))]
     for count in (n, n, nt, n, nk, nk, nk, nk, n, n):
-        scratch += [dma((count,)), dma((count,))]
+        sems += [dma((count,)), dma((count,))]
+
+    def scoped(*refs):
+        pl.run_scoped(functools.partial(layer_kernel, nk, nt, *refs), *sems)
+
     return pl.pallas_call(
-        functools.partial(layer_kernel, nk, nt),
-        out_shape=jax.ShapeDtypeStruct(resid.shape, resid.dtype),
+        scoped,
+        out_shape=pltpu.VMEM(resid.shape, resid.dtype),
         in_specs=[pl.BlockSpec(memory_space=pl.ANY)] * len(args),
         out_specs=pl.BlockSpec(memory_space=pltpu.VMEM),
         scratch_shapes=scratch,

time: 36.5 us -> 34 us (0.932)
  Pallas kernels: 35.1 us -> 33.3 us
  local copies, waits for them, and re-layouts: 1.26 us -> 0.58 us
    pallas_call x1, Pallas kernels: 35.1 us -> 33.3 us  [fused_layer(): pl.pallas_call(scoped, out_shape=pltpu.VMEM(resid.shape, resid.dtype), in...]
    unnamed x1, local copies, waits for them, and re-layouts: 1.26 us -> 0.58 us
where the time goes in v1:
time: 34 us; the launch traced here: 33.8 us
  Pallas kernels  33.3 us (98%)
  local copies, waits for them, and re-layouts  0.58 us (2%)
    pallas_call x1, Pallas kernels, fused_layer(): pl.pallas_call(scoped, out_shape=pltpu.VMEM(resid.shape, resid.dtype), in...  33.3 us

profile of v1, /device:TPU:0, one launch (start us, length us, event | category | flops | bytes accessed | tf_op | source)
XLA Modules:
  0.0 33.8 jit_solution(3869077545607000765)
XLA Ops:
  0.0 33.3 %shard_map.172 = bf16[4,256]{1,0:T(4,128)(2,1)S(1)} custom-call(bf16[4,256]{1,0:T(4,128)(2,1)} %refs_0_.1, bf16[3,256]{1,0:T(4,128)(2,1)} %refs_1_.1, bf16[2,704,2048]{2,1,0:T(8,128)(2,1)} %bitcast.21, bf16[2,704,2048]{2,1,0:T(8,128)(2,1)} %bitcast.22, bf16[2,704,2048]{2,1,0:T(8,128)(2,1)} %refs_4_.1, bf16[512,2048]{1,0:T(8,128)(2,1)} %bitcast.23, ...), custom_call_target="tpu_custom_call" | custom-call | tf_op jit(solution)/shard_map/pallas_call | solution.py:723
  33.3 0.6 %copy.20 = bf16[4,256]{1,0:T(4,128)(2,1)} copy(bf16[4,256]{1,0:T(4,128)(2,1)S(1)} %shard_map.172) | data formatting | bytes 4096

commit v2 on v1

v2 whole, which is shorter than its diff:
```python
from types import SimpleNamespace

import jax
import jax.numpy as jnp
from jax import lax
from jax.experimental import pallas as pl
from jax.experimental.pallas import tpu as pltpu
from jax.sharding import PartitionSpec as P

D = 2048
F32 = jnp.float32
BF16 = jnp.bfloat16
MESH = pl.DeviceIdType.MESH

EPS = 1e-06


def normalize(rows, gain):
    values = rows.astype(jnp.float32)
    scale = lax.rsqrt(jnp.mean(values * values, axis=1, keepdims=True) + EPS)
    return (values * scale * gain.astype(jnp.float32).reshape(1, -1)).astype(jnp.bfloat16)


def feed_forward(normed, w_gate, w_up, w_down):
    gate = jnp.dot(normed, w_gate, preferred_element_type=jnp.float32)
    upper = jnp.dot(normed, w_up, preferred_element_type=jnp.float32)
    hidden = (jax.nn.silu(gate) * upper).astype(jnp.bfloat16)
    return jnp.dot(hidden, w_down, preferred_element_type=jnp.float32)


def add_half(base, sums):
    return (base.astype(jnp.float32) + 0.5 * sums).astype(jnp.bfloat16)


def ffn_totals(partial_value):
    return lax.psum(partial_value, ("kv", "tp"))


def short_conv(history, newest, taps):
    window = jnp.concatenate(
        [history.astype(jnp.float32), newest.astype(jnp.float32)[:, None]], axis=1
    )
    return jax.nn.silu(jnp.sum(window * taps.astype(jnp.float32)[None], axis=1))


def state_step(
    xs_new,
    zeta,
    bc_new,
    dt_raw,
    conv_x,
    conv_bc,
    ssm_state,
    conv_wx,
    conv_wbc,
    dt_bias,
    a_log,
    d_skip,
):
    xconv = short_conv(conv_x, xs_new, conv_wx)
    bconv = short_conv(conv_bc, bc_new, conv_wbc)
    heads = xconv.shape[1]
    groups = bconv.shape[2]
    bmat = jnp.repeat(bconv[:, 0], heads // groups, axis=1)
    cmat = jnp.repeat(bconv[:, 1], heads // groups, axis=1)
    step_size = jax.nn.softplus(dt_raw + dt_bias[None, :])
    decay = jnp.exp(-step_size * jnp.exp(a_log)[None, :])
    updated = (
        decay[:, :, None, None] * ssm_state
        + (step_size[:, :, None] * xconv)[..., None] * bmat[:, :, None, :]
    )
    mixed = (
        jnp.einsum("shpn,shn->shp", updated, cmat, precision=lax.Precision.HIGHEST)
        + d_skip[None, :, None] * xconv
    )
    return (mixed * jax.nn.silu(zeta.astype(jnp.float32))).astype(jnp.bfloat16)


def group_terms(slab, w_bc, w_dt):
    span = slab.shape[1]
    flat_bc = w_bc.reshape(span, -1)
    bc_part = jnp.dot(slab, flat_bc, preferred_element_type=jnp.float32)
    dt_part = jnp.dot(slab, w_dt, preferred_element_type=jnp.float32)
    return (
        lax.psum_scatter(bc_part, "kv", scatter_dimension=0, tiled=True),
        lax.psum_scatter(dt_part, "kv", scatter_dimension=0, tiled=True),
    )


def mix_partial(
    normed,
    w_x,
    w_z,
    w_bc,
    w_dt,
    dt_bias,
    a_log,
    d_skip,
    conv_wx,
    conv_wbc,
    conv_x,
    conv_bc,
    ssm_state,
    w_out,
):
    rows = normed.shape[0]
    local_heads = w_x.shape[1]
    half = w_x.shape[2]
    xs_part = (
        jnp.dot(normed, w_x.reshape(D, -1), preferred_element_type=jnp.float32)
        .astype(jnp.bfloat16)
        .reshape(rows, local_heads, half)
    )
    zeta_part = (
        jnp.dot(normed, w_z.reshape(D, -1), preferred_element_type=jnp.float32)
        .astype(jnp.bfloat16)
        .reshape(rows, local_heads, half)
    )
    xs_new, zeta = (
        lax.all_to_all(xs_part, "kv", split_axis=0, concat_axis=1, tiled=True),
        lax.all_to_all(zeta_part, "kv", split_axis=0, concat_axis=1, tiled=True),
    )
    span = w_bc.shape[0]
    slab = lax.dynamic_slice_in_dim(normed, lax.axis_index("kv") * span, span, 1)
    bc_sum, dt_raw = group_terms(slab, w_bc, w_dt)
    bc_new = bc_sum.astype(jnp.bfloat16).reshape((bc_sum.shape[0],) + w_bc.shape[1:])
    mixed = state_step(
        xs_new,
        zeta,
        bc_new,
        dt_raw,
        conv_x,
        conv_bc,
        ssm_state,
        conv_wx,
        conv_wbc,
        dt_bias,
        a_log,
        d_skip,
    )
    flat_out = w_out.reshape(-1, w_out.shape[2])
    piece = lax.all_gather(mixed, "kv", axis=0, tiled=True)
    return jnp.dot(piece.reshape(piece.shape[0], -1), flat_out, preferred_element_type=jnp.float32)


def per_device(
    resid,
    norm_gain,
    ffn_gate,
    ffn_up,
    ffn_down,
    w_x,
    w_z,
    w_bc,
    w_dt,
    dt_bias,
    a_log,
    d_skip,
    conv_wx,
    conv_wbc,
    conv_x,
    conv_bc,
    ssm_state,
    w_out,
):
    mixer_args = (
        w_x,
        w_z,
        w_bc,
        w_dt,
        dt_bias,
        a_log,
        d_skip,
        conv_wx,
        conv_wbc,
        conv_x,
        conv_bc,
        ssm_state,
        w_out,
    )
    rows, gains = (
        lax.all_gather(resid, ("kv", "tp"), axis=1, tiled=True),
        lax.all_gather(norm_gain, ("kv", "tp"), axis=1, tiled=True),
    )
    first = add_half(
        rows,
        ffn_totals(feed_forward(normalize(rows, gains[0]), ffn_gate[0], ffn_up[0], ffn_down[0])),
    )
    partial_value = mix_partial(normalize(first, gains[1]), *mixer_args)
    span = partial_value.shape[1]
    block = lax.dynamic_slice_in_dim(first, lax.axis_index("kv") * span, span, 1)
    joined = (block.astype(jnp.float32) + lax.psum(partial_value, "tp")).astype(jnp.bfloat16)
    second = lax.all_gather(joined, "kv", axis=1, tiled=True)
    final = add_half(
        second,
        ffn_totals(feed_forward(normalize(second, gains[2]), ffn_gate[1], ffn_up[1], ffn_down[1])),
    )
    width = resid.shape[1]
    return lax.dynamic_slice_in_dim(final, lax.axis_index(("kv", "tp")) * width, width, 1)


def nt_dot(left, right):
    return lax.dot_general(left, right, (((1,), (1,)), ((), ())), preferred_element_type=F32)


def nn_dot(left, right):
    return jnp.dot(left, right, preferred_element_type=F32)


def silu(value):
    return value * jax.nn.sigmoid(value)


def norm_rows(values, gain):
    scale = lax.rsqrt(jnp.mean(values * values, axis=1, keepdims=True) + EPS)
    return (values * scale * gain).astype(BF16)


def split_two(value):
    high = value.astype(BF16)
    return high, (value - high.astype(F32)).astype(BF16)


def layer_kernel(
    nk,
    nt,
    resid,
    gains,
    gate,
    up,
    down,
    wx,
    wz,
    wbc,
    wdt,
    dt_bias,
    a_log,
    d_skip,
    cwx,
    cwbc,
    cx,
    cbc,
    state,
    wout,
    out,
    v,
    m,
):
    me_k, me_t = lax.axis_index("kv"), lax.axis_index("tp")
    n = nk * nt
    me = me_k * nt + me_t
    lead = nt - 1
    rows, width = resid.shape
    dim = n * width
    block = nt * width
    scope = jax.named_scope

    def target(index):
        return {"kv": lax.div(index, nt), "tp": lax.rem(index, nt)}

    def flipped(index, mask):
        bit = 1
        while bit < nk:
            if mask & bit:
                index = index + bit - 2 * bit * lax.rem(lax.div(index, bit), 2)
            bit *= 2
        return index

    def all_peers():
        order = [(x, d) for x in range(nk) for d in range(nt)][1:]
        return [flipped(me_k, x) * nt + lax.rem(me_t + d, nt) for x, d in order]

    def kv_peers():
        return [flipped(me_k, x) for x in range(1, nk)]

    loads = {}

    def load(name, src, dst):
        copy = pltpu.make_async_copy(src, dst, m.load.at[len(loads)])
        copy.start()
        loads[name] = copy

    def loaded(*names):
        with scope("w_" + names[0]):
            for name in names:
                loads[name].wait()

    load("rows", resid, v.rows.at[me])
    load("gains", gains, v.gain.at[me])
    barrier = pltpu.get_barrier_semaphore()
    for q in all_peers()[::-1]:
        pl.semaphore_signal(barrier, inc=1, device_id=target(q), device_id_type=MESH)
    load("gate0", gate.at[0], v.gate.at[0])
    load("up0", up.at[0], v.up.at[0])
    load("down0", down.at[0], v.down.at[0])
    load("wbc", wbc, v.wbc)
    load("bias", dt_bias, v.small.at[0])
    load("alog", a_log, v.small.at[1])
    load("skip", d_skip, v.small.at[2])
    load("cwx", cwx, v.cwx)
    load("cwbc", cwbc, v.cwbc)
    load("cx", cx, v.cx)
    load("cbc", cbc, v.cbc)
    load("wdt", wdt, v.wdt)
    load("state", state, v.state)
    load("wx", wx, v.wx)
    load("wz", wz, v.wz)
    load("wout", wout, v.wout)
    load("gate1", gate.at[1], v.gate.at[1])
    load("up1", up.at[1], v.up.at[1])
    load("down1", down.at[1], v.down.at[1])
    with scope("w_barrier"):
        pl.semaphore_wait(barrier, n - 1)

    def remote(src, dst, ssem, rsem, index):
        return pltpu.make_async_remote_copy(
            src_ref=src,
            dst_ref=dst,
            send_sem=ssem,
            recv_sem=rsem,
            device_id=target(index),
            device_id_type=MESH,
        )

    sent = []

    def send(src, dst, ssem, rsem, index):
        copy = remote(src, dst, ssem, rsem, index)
        copy.start()
        sent.append(copy)

    def arrived(slots, sems, slot, index):
        remote(slots.at[slot], slots.at[slot], sems[0].at[slot], sems[1].at[slot], index).wait_recv()

    loaded("rows", "gains")
    for q in all_peers()[::-1]:
        send(v.rows.at[me], v.rows.at[me], m.rows[0].at[q], m.rows[1].at[me], q)
    for q in all_peers()[::-1]:
        send(v.gain.at[me], v.gain.at[me], m.gain[0].at[q], m.gain[1].at[me], q)

    heads, half = v.cx.shape[2], v.cx.shape[1]
    flat = heads * half
    groups = v.cwbc.shape[1] // 2
    pairs = 2 * groups
    lane = lax.broadcasted_iota(jnp.int32, v.expand.shape, 1)
    head_of = lax.broadcasted_iota(jnp.int32, v.expand.shape, 0) * half
    v.expand[...] = jnp.where((lane >= head_of) & (lane < head_of + half), 1.0, 0.0).astype(BF16)
    tile = v.perm.shape[0]
    deep = tile // pairs
    row = lax.broadcasted_iota(jnp.int32, v.perm.shape, 0)
    lane = lax.broadcasted_iota(jnp.int32, v.perm.shape, 1)
    source = (row & (deep - 1)) * pairs + lax.shift_right_logical(row, deep.bit_length() - 1)
    v.perm[...] = jnp.where(lane == source, 1.0, 0.0).astype(BF16)

    units = v.gate.shape[1]

    def gated(blocks, which):
        squares = jnp.zeros((rows, 1), F32)
        g = jnp.zeros((rows, units), F32)
        u = jnp.zeros((rows, units), F32)
        for values, gain, at in blocks:
            squares = squares + jnp.sum(values * values, axis=1, keepdims=True)
            left = (values * gain).astype(BF16)
            g = g + nt_dot(left, v.gate[which, :, at])
            u = u + nt_dot(left, v.up[which, :, at])
        scale = lax.rsqrt(squares / dim + EPS)
        return (silu(g * scale) * (u * scale)).astype(BF16)

    def columns(index, count):
        return pl.ds(pl.multiple_of(index * count, 128), count)

    def arriving_rows():
        for q in [me] + all_peers():
            if q is not me:
                with scope("w_rows"):
                    arrived(v.rows, m.rows, q, q)
                    arrived(v.gain, m.gain, q, q)
            yield v.rows[q].astype(F32), v.gain[q, 0:1, :].astype(F32), columns(q, width)

    loaded("gate0", "up0")
    hidden = gated(arriving_rows(), 0)
    loaded("down0")
    for x in range(nk)[::-1]:
        k = flipped(me_k, x)
        v.part[k] = nn_dot(hidden, v.down[0, :, columns(k, block)]).astype(BF16)
        for d in range(nt)[::-1]:
            t = (lead + nt - d) % nt if x else lax.rem(me_t + d, nt)
            if x or d:
                q = k * nt + t
                send(v.part.at[k], v.slab.at[me], m.slab[0].at[q], m.slab[1].at[me], q)
    v.slab[me] = v.part[me_k]
    for q in all_peers()[::-1]:
        send(v.part, v.full.at[me], m.full[0].at[q], m.full[1].at[me], q)

    def gain_cut(index, i):
        return jnp.concatenate(
            [v.gain[index * nt + t, i : i + 1, :].astype(F32) for t in range(nt)], axis=1
        )

    def rows_cut(index):
        return jnp.concatenate([v.rows[index * nt + t].astype(F32) for t in range(nt)], axis=1)

    def expand(value):
        return nn_dot(value, v.expand[...])

    loaded("wbc")
    span = v.wdt.shape[1]
    for c in range(span // deep):
        piece = nn_dot(v.perm[...], v.wbc[c * tile : (c + 1) * tile, :]).astype(BF16)
        for p in range(pairs):
            v.wide[c * deep : (c + 1) * deep, p * 128 : (p + 1) * 128] = piece[
                p * deep : (p + 1) * deep, :
            ]

    loaded("bias", "alog", "skip", "cwx", "cwbc", "cx", "cbc")
    taps = v.cx.shape[0]
    known = sum(v.cx[i].astype(F32) * v.cwx[i].astype(F32) for i in range(taps))
    high, low = split_two(known)
    lane = lax.broadcasted_iota(jnp.int32, (half, flat), 1)
    row = lax.broadcasted_iota(jnp.int32, (half, flat), 0)
    own = (lane & (half - 1)) == row
    v.hist[me_k] = jnp.sum(jnp.where(own, expand(high) + expand(low), 0.0), axis=0, keepdims=True)
    for k in kv_peers()[::-1]:
        q = k * nt + me_t
        send(v.hist.at[me_k], v.hist.at[me_k], m.hist[0].at[k], m.hist[1].at[me_k], q)
    tap_x = jnp.sum(jnp.where(own, expand(v.cwx[taps]), 0.0), axis=0, keepdims=True)
    skip_high, skip_low = split_two(v.small[2])
    v.line[0] = tap_x
    v.line[1] = expand(skip_high) + expand(skip_low)
    hist_bc = sum(v.cbc[i].astype(F32) * v.cwbc[i].astype(F32) for i in range(taps))
    tap_bc = v.cwbc[taps].astype(F32)
    loaded("state", "wdt")
    v.state_b[...] = v.state[...].astype(BF16)

    with scope("w_slab"):
        for q in all_peers():
            arrived(v.slab, m.slab, q, q)
    total = sum(v.slab[q].astype(F32) for q in range(n))
    near = (rows_cut(me_k) + 0.5 * total).astype(BF16).astype(F32)
    left = (near * gain_cut(me_k, 1)).astype(BF16)
    bc_part = nn_dot(left, v.wide[...])
    dt_part = nt_dot(left, v.wdt[...])
    tall = v.bc.shape[1]
    for p in range(pairs):
        v.bc_b[pl.ds(p, rows, stride=tall), :] = bc_part[:, p * 128 : (p + 1) * 128]
    v.bc_b[pl.ds(pairs, rows, stride=tall), :] = jnp.concatenate(
        [dt_part, jnp.zeros((rows, 128 - heads), F32)], axis=1
    )

    def bc_row(k):
        return v.bc_b.at[pl.ds(pl.multiple_of(k * tall, 8), tall), :]

    def bc_sends():
        for k in kv_peers()[::-1]:
            for t in range(nt):
                q = k * nt + t
                yield remote(bc_row(k), v.bc.at[me_k], m.bc[0].at[q], m.bc[1].at[me_k], q)

    @pl.when(me_t == lead)
    def _():
        for copy in bc_sends():
            copy.start()

    with scope("w_full"):
        for q in all_peers():
            arrived(v.full, m.full, q, q)
    squares = jnp.zeros((rows, 1), F32)
    v.full[me] = v.part[...]
    for k in range(nk):
        total = sum(v.full[q, k].astype(F32) for q in range(n))
        first = (rows_cut(k) + 0.5 * total).astype(BF16).astype(F32)
        v.first[k] = first
        v.xn[k] = (first * gain_cut(k, 1)).astype(BF16)
        squares = squares + jnp.sum(first * first, axis=1, keepdims=True)
    scale = lax.rsqrt(squares / dim + EPS)
    v.scale[...] = jnp.broadcast_to(scale, v.scale.shape)

    loaded("wx", "wz")
    local = v.wx.shape[0]
    xs_part = jnp.zeros((rows, local), F32)
    z_part = jnp.zeros((rows, local), F32)
    for k in range(nk):
        xs_part = xs_part + nt_dot(v.xn[k], v.wx[:, k * block : (k + 1) * block])
        z_part = z_part + nt_dot(v.xn[k], v.wz[:, k * block : (k + 1) * block])
    v.xz[me_k] = jnp.concatenate([xs_part * scale, z_part * scale], axis=1).astype(BF16)
    for k in kv_peers()[::-1]:
        q = k * nt + me_t
        send(v.xz.at[me_k], v.xz.at[me_k], m.xz[0].at[k], m.xz[1].at[me_k], q)

    with scope("w_bc"):
        for k in kv_peers():
            arrived(v.bc, m.bc, k, k * nt + lead)
    v.bc[me_k] = bc_row(me_k)[...]
    summed = sum(v.bc[k] for k in range(nk)) * v.scale[pl.ds(me_k, 1), :]
    raw = summed[pairs : pairs + 1, :heads] + v.small[0]
    step = jnp.maximum(raw, 0.0) + jnp.log1p(jnp.exp(-jnp.abs(raw)))
    decay = jnp.exp(-step * jnp.exp(v.small[1]))
    step_high, step_low = split_two(step)
    decay_high, decay_low = split_two(decay)
    spread = expand(jnp.concatenate([decay_high, decay_low, step_high, step_low], axis=0))
    decay_row = spread[0:1] + spread[1:2]
    step_row = spread[2:3] + spread[3:4]
    bc_new = summed[:pairs].astype(BF16).astype(F32)
    bconv = silu(hist_bc + bc_new * tap_bc)
    bmat, cmat = bconv[:groups], bconv[groups:]
    weight = jnp.sum(bmat * cmat, axis=1, keepdims=True)
    per_group = nt_dot(cmat.astype(BF16), v.state_b[...])
    lane = lax.broadcasted_iota(jnp.int32, (groups, flat), 1)
    low_end = lax.broadcasted_iota(jnp.int32, (groups, flat), 0) * (flat // groups)
    mine = (lane >= low_end) & (lane < low_end + flat // groups)
    read = jnp.sum(jnp.where(mine, per_group, 0.0), axis=0, keepdims=True)
    cross = jnp.sum(jnp.where(mine, weight, 0.0), axis=0, keepdims=True)
    v.mix[me_k] = jnp.concatenate(
        [decay_row * read, step_row * cross + v.line[1]], axis=0
    ).astype(BF16)
    for k in kv_peers()[::-1]:
        q = k * nt + me_t
        send(v.mix.at[me_k], v.mix.at[me_k], m.mix[0].at[k], m.mix[1].at[me_k], q)

    with scope("w_xz"):
        for k in kv_peers():
            arrived(v.hist, m.hist, k, k * nt + me_t)
            arrived(v.xz, m.xz, k, k * nt + me_t)
    for k in range(nk):
        at = slice(k * local, (k + 1) * local)
        past = jnp.concatenate([v.hist[i][:, at] for i in range(nk)], axis=0)
        v.xconv[:, at] = silu(past + v.xz[k][:, :local].astype(F32) * v.line[0][:, at])
        v.open[:, at] = silu(v.xz[k][:, local:].astype(F32))
    loaded("wout")
    with scope("w_mix"):
        for k in kv_peers():
            arrived(v.mix, m.mix, k, k * nt + me_t)
    pieces = [v.mix[k].astype(F32) for k in range(nk)]
    read = jnp.concatenate([piece[0:1] for piece in pieces], axis=0)
    direct = jnp.concatenate([piece[1:2] for piece in pieces], axis=0)
    mixed = ((read + direct * v.xconv[...]) * v.open[...]).astype(BF16)
    v.proj[me] = nn_dot(mixed, v.wout[...]).astype(BF16)
    for q in all_peers()[::-1]:
        send(v.proj.at[me], v.proj.at[me], m.proj[0].at[q], m.proj[1].at[me], q)

    def arriving_blocks():
        for x in range(nk):
            k = flipped(me_k, x)
            with scope("w_proj"):
                for d in range(nt):
                    if x or d:
                        q = k * nt + lax.rem(me_t + d, nt)
                        arrived(v.proj, m.proj, q, q)
            total = sum(v.proj[k * nt + t].astype(F32) for t in range(nt))
            second = (v.first[k] + total).astype(BF16).astype(F32)
            if x == 0:
                for t in range(nt):
                    v.second[t] = second[:, t * width : (t + 1) * width]
            yield second, gain_cut(k, 2), columns(k, block)

    loaded("gate1", "up1")
    hidden = gated(arriving_blocks(), 1)
    loaded("down1")
    for x in range(nk)[::-1]:
        k = flipped(me_k, x)
        piece = nn_dot(hidden, v.down[1, :, columns(k, block)])
        for t in range(nt):
            v.cut_b[k * nt + t] = piece[:, t * width : (t + 1) * width].astype(BF16)
        for d in range(nt)[::-1]:
            if x or d:
                q = k * nt + lax.rem(me_t + d, nt)
                send(v.cut_b.at[q], v.cut.at[me], m.cut[0].at[q], m.cut[1].at[me], q)
    v.cut[me] = v.cut_b[me]
    with scope("w_cut"):
        for q in all_peers():
            arrived(v.cut, m.cut, q, q)
    total = sum(v.cut[q].astype(F32) for q in range(n))
    out[...] = (v.second[me_t] + 0.5 * total).astype(BF16)
    with scope("w_sent"):
        for copy in sent:
            copy.wait_send()

        @pl.when(me_t == lead)
        def _():
            for copy in bc_sends():
                copy.wait_send()


def fused_layer(
    nk,
    nt,
    resid,
    norm_gain,
    ffn_gate,
    ffn_up,
    ffn_down,
    w_x,
    w_z,
    w_bc,
    w_dt,
    dt_bias,
    a_log,
    d_skip,
    conv_wx,
    conv_wbc,
    conv_x,
    conv_bc,
    ssm_state,
    w_out,
):
    n = nk * nt
    rows, width = resid.shape
    dim = ffn_gate.shape[1]
    units = ffn_gate.shape[2]
    local = w_x.shape[1] * w_x.shape[2]
    heads, half = conv_x.shape[2], conv_x.shape[3]
    flat = heads * half
    span = w_bc.shape[0]
    lanes = w_bc.shape[3]
    pairs = w_bc.shape[1] * w_bc.shape[2]
    out_cols = w_out.shape[2]
    taps = conv_wx.shape[0]
    block = nt * width
    args = (
        resid,
        norm_gain,
        jnp.swapaxes(ffn_gate, 1, 2),
        jnp.swapaxes(ffn_up, 1, 2),
        ffn_down,
        jnp.transpose(w_x, (1, 2, 0)).reshape(local, dim),
        jnp.transpose(w_z, (1, 2, 0)).reshape(local, dim),
        w_bc.reshape(span * pairs, lanes),
        w_dt.T,
        dt_bias.reshape(1, heads),
        a_log.reshape(1, heads),
        d_skip.reshape(1, heads),
        jnp.swapaxes(conv_wx, 1, 2),
        conv_wbc.reshape(taps, pairs, lanes),
        jnp.swapaxes(conv_x, 2, 3).reshape(taps - 1, half, heads),
        conv_bc.reshape(taps - 1, pairs, lanes),
        ssm_state.reshape(flat, lanes),
        w_out.reshape(flat, out_cols),
    )
    dma = pltpu.SemaphoreType.DMA
    vmem = pltpu.VMEM
    scratch = dict(
        gate=vmem((2, units, dim), BF16),
        up=vmem((2, units, dim), BF16),
        down=vmem((2, units, dim), BF16),
        wx=vmem((local, dim), BF16),
        wz=vmem((local, dim), BF16),
        wbc=vmem((span * pairs, lanes), BF16),
        wide=vmem((span, pairs * lanes), BF16),
        wdt=vmem((heads, span), BF16),
        state=vmem((flat, lanes), F32),
        state_b=vmem((flat, lanes), BF16),
        wout=vmem((flat, out_cols), BF16),
        small=vmem((3, 1, heads), F32),
        cwx=vmem((taps, half, heads), BF16),
        cwbc=vmem((taps, pairs, lanes), BF16),
        cx=vmem((taps - 1, half, heads), BF16),
        cbc=vmem((taps - 1, pairs, lanes), BF16),
        expand=vmem((heads, flat), BF16),
        perm=vmem((256, 256), BF16),
        rows=vmem((n, rows, width), BF16),
        gain=vmem((n, 3, width), BF16),
        part=vmem((nk, rows, block), BF16),
        slab=vmem((n, rows, block), BF16),
        full=vmem((n, nk, rows, block), BF16),
        first=vmem((nk, rows, block), F32),
        xn=vmem((nk, rows, block), BF16),
        scale=vmem((rows, lanes), F32),
        bc_b=vmem((nk * (pairs + 8), lanes), F32),
        bc=vmem((nk, pairs + 8, lanes), F32),
        hist=vmem((nk, 1, flat), F32),
        line=vmem((2, 1, flat), F32),
        xz=vmem((nk, rows, 2 * local), BF16),
        xconv=vmem((rows, flat), F32),
        open=vmem((rows, flat), F32),
        mix=vmem((nk, 2, flat), BF16),
        proj=vmem((n, rows, out_cols), BF16),
        second=vmem((nt, rows, width), F32),
        cut_b=vmem((n, rows, width), BF16),
        cut=vmem((n, rows, width), BF16),
    )
    rounds = dict(
        rows=n, gain=n, slab=n, full=n, bc=n, hist=nk, xz=nk, mix=nk, proj=n, cut=n
    )
    sems = {name: (dma((count,)), dma((count,))) for name, count in rounds.items()}
    sems["load"] = dma((21,))

    def kernel(*refs, **held):
        def body(**flags):
            layer_kernel(nk, nt, *refs, SimpleNamespace(**held), SimpleNamespace(**flags))

        pl.run_scoped(body, **sems)

    return pl.pallas_call(
        kernel,
        out_shape=pltpu.VMEM(resid.shape, resid.dtype),
        in_specs=[pl.BlockSpec(memory_space=pl.ANY)] * len(args),
        out_specs=pl.BlockSpec(memory_space=pltpu.VMEM),
        scratch_shapes=scratch,
        compiler_params=pltpu.CompilerParams(
            collective_id=0, has_side_effects=True, vmem_limit_bytes=60 * 1024 * 1024
        ),
    )(*args)


def fits(nk, nt, resid, w_x, w_bc, conv_x):
    rows, width = resid.shape
    half = conv_x.shape[3]
    pairs = w_bc.shape[1] * w_bc.shape[2]
    return (
        conv_x.shape[0] == 1
        and rows == nk
        and nt > 1
        and nk & (nk - 1) == 0
        and w_bc.shape[0] == nt * width
        and width % 128 == 0
        and w_bc.shape[0] % 128 == 0
        and (w_x.shape[1] * w_x.shape[2]) % 128 == 0
        and half & (half - 1) == 0
        and pairs & (pairs - 1) == 0
        and pairs % 8 == 0
        and 256 % pairs == 0
        and (w_bc.shape[0] * pairs) % 256 == 0
        and w_bc.shape[3] == 128
        and conv_x.shape[2] < 128
    )


def solution(mesh):
    placed = (
        P("dp", ("kv", "tp")),
        P(None, ("kv", "tp")),
        P(None, None, ("kv", "tp")),
        P(None, None, ("kv", "tp")),
        P(None, ("kv", "tp"), None),
        P(None, "kv", "tp"),
        P(None, "kv", "tp"),
        P("kv", None, None, None),
        P("kv", None),
        P(),
        P(),
        P(),
        P(None, None, "tp"),
        P(),
        P(("dp", "kv"), None, None, "tp"),
        P(("dp", "kv"), None, None, None, None),
        P(("dp", "kv"), None, "tp", None),
        P(None, "tp", "kv"),
    )
    nk, nt = mesh.shape["kv"], mesh.shape["tp"]

    def layer(*args):
        if fits(nk, nt, args[0], args[5], args[7], args[14]):
            return fused_layer(nk, nt, *args)
        return per_device(*args)

    return jax.shard_map(
        layer, mesh=mesh, in_specs=placed, out_specs=P("dp", ("kv", "tp")), check_vma=False
    )
```

time: 34 us -> 30.8 us (0.906)
  Pallas kernels: 33.3 us -> 30.1 us
    pallas_call x1, Pallas kernels: 33.3 us -> 30.1 us  [fused_layer(): pl.pallas_call(kernel, out_shape=pltpu.VMEM(resid.shape, resid.dtype), in...]
where the time goes in v2:
time: 30.8 us; the launch traced here: 30.7 us
  Pallas kernels  30.1 us (98%)
  local copies, waits for them, and re-layouts  0.58 us (2%)
    pallas_call x1, Pallas kernels, fused_layer(): pl.pallas_call(kernel, out_shape=pltpu.VMEM(resid.shape, resid.dtype), in...  30.1 us

profile of v2, /device:TPU:0, one launch (start us, length us, event | category | flops | bytes accessed | tf_op | source)
XLA Modules:
  0.0 30.7 jit_solution(4842678029706320994)
XLA Ops:
  0.0 30.1 %shard_map.172 = bf16[4,256]{1,0:T(4,128)(2,1)S(1)} custom-call(bf16[4,256]{1,0:T(4,128)(2,1)} %refs_0_.1, bf16[3,256]{1,0:T(4,128)(2,1)} %refs_1_.1, bf16[2,704,2048]{2,1,0:T(8,128)(2,1)} %bitcast.21, bf16[2,704,2048]{2,1,0:T(8,128)(2,1)} %bitcast.22, bf16[2,704,2048]{2,1,0:T(8,128)(2,1)} %refs_4_.1, bf16[512,2048]{1,0:T(8,128)(2,1)} %bitcast.23, ...), custom_call_target="tpu_custom_call" | custom-call | tf_op jit(solution)/shard_map/pallas_call | solution.py:693
  30.1 0.6 %copy.20 = bf16[4,256]{1,0:T(4,128)(2,1)} copy(bf16[4,256]{1,0:T(4,128)(2,1)S(1)} %shard_map.172) | data formatting | bytes 4096

commit v3 on v2

--- a/solution.py
+++ b/solution.py
@@ -290,10 +290,6 @@
     barrier = pltpu.get_barrier_semaphore()
     for q in all_peers()[::-1]:
         pl.semaphore_signal(barrier, inc=1, device_id=target(q), device_id_type=MESH)
-    load("gate0", gate.at[0], v.gate.at[0])
-    load("up0", up.at[0], v.up.at[0])
-    load("down0", down.at[0], v.down.at[0])
-    load("wbc", wbc, v.wbc)
     load("bias", dt_bias, v.small.at[0])
     load("alog", a_log, v.small.at[1])
     load("skip", d_skip, v.small.at[2])
@@ -301,11 +297,31 @@
     load("cwbc", cwbc, v.cwbc)
     load("cx", cx, v.cx)
     load("cbc", cbc, v.cbc)
-    load("wdt", wdt, v.wdt)
-    load("state", state, v.state)
+    load("gate0", gate.at[0], v.gate.at[0])
+    load("up0", up.at[0], v.up.at[0])
+    load("down0", down.at[0], v.down.at[0])
+    lead_loads = (
+        (wbc, v.wbc),
+        (wdt, v.wdt),
+        (state, v.state.at[lead]),
+        (wout, v.wout.at[lead]),
+    )
+
+    def lead_load(i):
+        return pltpu.make_async_copy(*lead_loads[i], m.lead.at[i])
+
+    @pl.when(me_t == lead)
+    def _():
+        for i in range(3):
+            lead_load(i).start()
+
     load("wx", wx, v.wx)
     load("wz", wz, v.wz)
-    load("wout", wout, v.wout)
+
+    @pl.when(me_t == lead)
+    def _():
+        lead_load(3).start()
+
     load("gate1", gate.at[1], v.gate.at[1])
     load("up1", up.at[1], v.up.at[1])
     load("down1", down.at[1], v.down.at[1])
@@ -337,6 +353,17 @@
         send(v.rows.at[me], v.rows.at[me], m.rows[0].at[q], m.rows[1].at[me], q)
     for q in all_peers()[::-1]:
         send(v.gain.at[me], v.gain.at[me], m.gain[0].at[q], m.gain[1].at[me], q)
+
+    home = me_k * nt + lead
+
+    def pushes():
+        yield remote(state, v.state.at[me_t], m.state[0].at[me_t], m.state[1].at[me_t], home)
+        yield remote(wout, v.wout.at[me_t], m.wout[0].at[me_t], m.wout[1].at[me_t], home)
+
+    @pl.when(me_t != lead)
+    def _():
+        for copy in pushes():
+            copy.start()
 
     heads, half = v.cx.shape[2], v.cx.shape[1]
     flat = heads * half
@@ -352,17 +379,67 @@
     source = (row & (deep - 1)) * pairs + lax.shift_right_logical(row, deep.bit_length() - 1)
     v.perm[...] = jnp.where(lane == source, 1.0, 0.0).astype(BF16)
 
+    def expand(value):
+        return nn_dot(value, v.expand[...])
+
+    loaded("bias", "alog", "skip", "cwx", "cwbc", "cx", "cbc")
+    taps = v.cx.shape[0]
+    known = sum(v.cx[i].astype(F32) * v.cwx[i].astype(F32) for i in range(taps))
+    high, low = split_two(known)
+    lane = lax.broadcasted_iota(jnp.int32, (half, flat), 1)
+    row = lax.broadcasted_iota(jnp.int32, (half, flat), 0)
+    own = (lane & (half - 1)) == row
+    v.hist[me_k, me_t] = jnp.sum(
+        jnp.where(own, expand(high) + expand(low), 0.0), axis=0, keepdims=True
+    )
+    v.tap[me_t] = jnp.sum(jnp.where(own, expand(v.cwx[taps]), 0.0), axis=0, keepdims=True)
+    skip_high, skip_low = split_two(v.small[2])
+    v.line[...] = expand(skip_high) + expand(skip_low)
+
+    def to_leads(ref, sems):
+        for k in kv_peers()[::-1]:
+            q = k * nt + lead
+            yield remote(ref.at[me_k, me_t], ref.at[me_k, me_t], sems[0].at[k], sems[1].at[me], q)
+
+    def to_home(ref, sems):
+        return remote(
+            ref.at[me_k, me_t], ref.at[me_k, me_t], sems[0].at[me_k], sems[1].at[me], home
+        )
+
+    def tap_home():
+        return remote(v.tap.at[me_t], v.tap.at[me_t], m.tap[0].at[me_t], m.tap[1].at[me_t], home)
+
+    for copy in to_leads(v.hist, m.hist):
+        copy.start()
+        sent.append(copy)
+
+    @pl.when(me_t != lead)
+    def _():
+        to_home(v.hist, m.hist).start()
+        tap_home().start()
+
+    hist_bc = sum(v.cbc[i].astype(F32) * v.cwbc[i].astype(F32) for i in range(taps))
+    tap_bc = v.cwbc[taps].astype(F32)
+
     units = v.gate.shape[1]
 
-    def gated(blocks, which):
+    def gated(blocks, which, kept):
         squares = jnp.zeros((rows, 1), F32)
         g = jnp.zeros((rows, units), F32)
         u = jnp.zeros((rows, units), F32)
-        for values, gain, at in blocks:
+        for step, (values, gain, at) in enumerate(blocks):
             squares = squares + jnp.sum(values * values, axis=1, keepdims=True)
             left = (values * gain).astype(BF16)
             g = g + nt_dot(left, v.gate[which, :, at])
             u = u + nt_dot(left, v.up[which, :, at])
+            if step < kept:
+                v.held[step, 0] = g
+                v.held[step, 1] = u
+                g = jnp.zeros((rows, units), F32)
+                u = jnp.zeros((rows, units), F32)
+        for step in range(kept):
+            g = g + v.held[step, 0]
+            u = u + v.held[step, 1]
         scale = lax.rsqrt(squares / dim + EPS)
         return (silu(g * scale) * (u * scale)).astype(BF16)
 
@@ -378,19 +455,22 @@
             yield v.rows[q].astype(F32), v.gain[q, 0:1, :].astype(F32), columns(q, width)
 
     loaded("gate0", "up0")
-    hidden = gated(arriving_rows(), 0)
+    hidden = gated(arriving_rows(), 0, 0)
     loaded("down0")
     for x in range(nk)[::-1]:
         k = flipped(me_k, x)
         v.part[k] = nn_dot(hidden, v.down[0, :, columns(k, block)]).astype(BF16)
-        for d in range(nt)[::-1]:
-            t = (lead + nt - d) % nt if x else lax.rem(me_t + d, nt)
-            if x or d:
-                q = k * nt + t
-                send(v.part.at[k], v.slab.at[me], m.slab[0].at[q], m.slab[1].at[me], q)
-    v.slab[me] = v.part[me_k]
-    for q in all_peers()[::-1]:
-        send(v.part, v.full.at[me], m.full[0].at[q], m.full[1].at[me], q)
+        q = k * nt + lead
+        if x:
+            send(v.part.at[k], v.slab.at[me], m.slab[0].at[q], m.slab[1].at[me], q)
+
+    def slab_home():
+        q = me_k * nt + lead
+        return remote(v.part.at[me_k], v.slab.at[me], m.slab[0].at[q], m.slab[1].at[me], q)
+
+    @pl.when(me_t != lead)
+    def _():
+        slab_home().start()
 
     def gain_cut(index, i):
         return jnp.concatenate(
@@ -400,161 +480,194 @@
     def rows_cut(index):
         return jnp.concatenate([v.rows[index * nt + t].astype(F32) for t in range(nt)], axis=1)
 
-    def expand(value):
-        return nn_dot(value, v.expand[...])
-
-    loaded("wbc")
-    span = v.wdt.shape[1]
-    for c in range(span // deep):
-        piece = nn_dot(v.perm[...], v.wbc[c * tile : (c + 1) * tile, :]).astype(BF16)
-        for p in range(pairs):
-            v.wide[c * deep : (c + 1) * deep, p * 128 : (p + 1) * 128] = piece[
-                p * deep : (p + 1) * deep, :
-            ]
-
-    loaded("bias", "alog", "skip", "cwx", "cwbc", "cx", "cbc")
-    taps = v.cx.shape[0]
-    known = sum(v.cx[i].astype(F32) * v.cwx[i].astype(F32) for i in range(taps))
-    high, low = split_two(known)
-    lane = lax.broadcasted_iota(jnp.int32, (half, flat), 1)
-    row = lax.broadcasted_iota(jnp.int32, (half, flat), 0)
-    own = (lane & (half - 1)) == row
-    v.hist[me_k] = jnp.sum(jnp.where(own, expand(high) + expand(low), 0.0), axis=0, keepdims=True)
-    for k in kv_peers()[::-1]:
-        q = k * nt + me_t
-        send(v.hist.at[me_k], v.hist.at[me_k], m.hist[0].at[k], m.hist[1].at[me_k], q)
-    tap_x = jnp.sum(jnp.where(own, expand(v.cwx[taps]), 0.0), axis=0, keepdims=True)
-    skip_high, skip_low = split_two(v.small[2])
-    v.line[0] = tap_x
-    v.line[1] = expand(skip_high) + expand(skip_low)
-    hist_bc = sum(v.cbc[i].astype(F32) * v.cwbc[i].astype(F32) for i in range(taps))
-    tap_bc = v.cwbc[taps].astype(F32)
-    loaded("state", "wdt")
-    v.state_b[...] = v.state[...].astype(BF16)
-
-    with scope("w_slab"):
-        for q in all_peers():
-            arrived(v.slab, m.slab, q, q)
-    total = sum(v.slab[q].astype(F32) for q in range(n))
-    near = (rows_cut(me_k) + 0.5 * total).astype(BF16).astype(F32)
-    left = (near * gain_cut(me_k, 1)).astype(BF16)
-    bc_part = nn_dot(left, v.wide[...])
-    dt_part = nt_dot(left, v.wdt[...])
     tall = v.bc.shape[1]
-    for p in range(pairs):
-        v.bc_b[pl.ds(p, rows, stride=tall), :] = bc_part[:, p * 128 : (p + 1) * 128]
-    v.bc_b[pl.ds(pairs, rows, stride=tall), :] = jnp.concatenate(
-        [dt_part, jnp.zeros((rows, 128 - heads), F32)], axis=1
-    )
 
     def bc_row(k):
         return v.bc_b.at[pl.ds(pl.multiple_of(k * tall, 8), tall), :]
 
+    def first_sends():
+        for q in all_peers()[::-1]:
+            yield remote(v.near.at[me_k], v.near.at[me_k], m.near[0].at[q], m.near[1].at[me_k], q)
+
     def bc_sends():
         for k in kv_peers()[::-1]:
-            for t in range(nt):
-                q = k * nt + t
-                yield remote(bc_row(k), v.bc.at[me_k], m.bc[0].at[q], m.bc[1].at[me_k], q)
+            q = k * nt + lead
+            yield remote(bc_row(k), v.bc.at[me_k], m.bc[0].at[k], m.bc[1].at[me_k], q)
 
     @pl.when(me_t == lead)
     def _():
+        with scope("w_wbc"):
+            lead_load(0).wait()
+            lead_load(1).wait()
+        span = v.wdt.shape[1]
+        for c in range(span // deep):
+            piece = nn_dot(v.perm[...], v.wbc[c * tile : (c + 1) * tile, :]).astype(BF16)
+            for p in range(pairs):
+                v.wide[c * deep : (c + 1) * deep, p * 128 : (p + 1) * 128] = piece[
+                    p * deep : (p + 1) * deep, :
+                ]
+        v.slab[me] = v.part[me_k]
+        with scope("w_slab"):
+            for q in all_peers():
+                arrived(v.slab, m.slab, q, q)
+        total = sum(v.slab[q].astype(F32) for q in range(n))
+        first = (rows_cut(me_k) + 0.5 * total).astype(BF16)
+        v.near[me_k] = first
+        for copy in first_sends():
+            copy.start()
+        left = (first.astype(F32) * gain_cut(me_k, 1)).astype(BF16)
+        bc_part = nn_dot(left, v.wide[...])
+        dt_part = nt_dot(left, v.wdt[...])
+        for p in range(pairs):
+            v.bc_b[pl.ds(p, rows, stride=tall), :] = bc_part[:, p * 128 : (p + 1) * 128]
+        v.bc_b[pl.ds(pairs, rows, stride=tall), :] = jnp.concatenate(
+            [dt_part, jnp.zeros((rows, 128 - heads), F32)], axis=1
+        )
         for copy in bc_sends():
             copy.start()
-
-    with scope("w_full"):
-        for q in all_peers():
-            arrived(v.full, m.full, q, q)
-    squares = jnp.zeros((rows, 1), F32)
-    v.full[me] = v.part[...]
-    for k in range(nk):
-        total = sum(v.full[q, k].astype(F32) for q in range(n))
-        first = (rows_cut(k) + 0.5 * total).astype(BF16).astype(F32)
-        v.first[k] = first
-        v.xn[k] = (first * gain_cut(k, 1)).astype(BF16)
-        squares = squares + jnp.sum(first * first, axis=1, keepdims=True)
-    scale = lax.rsqrt(squares / dim + EPS)
-    v.scale[...] = jnp.broadcast_to(scale, v.scale.shape)
+        v.bc[me_k] = bc_row(me_k)[...]
+
+    def arrived_at(slots, sems, k, t):
+        q = k * nt + t
+        remote(slots.at[k, t], slots.at[k, t], sems[0].at[k], sems[1].at[q], q).wait_recv()
+
+    def arrived_from_lead(slots, sems, k):
+        @pl.when(k * nt + lead != me)
+        def _():
+            arrived(slots, sems, k, k * nt + lead)
 
     loaded("wx", "wz")
     local = v.wx.shape[0]
     xs_part = jnp.zeros((rows, local), F32)
     z_part = jnp.zeros((rows, local), F32)
-    for k in range(nk):
-        xs_part = xs_part + nt_dot(v.xn[k], v.wx[:, k * block : (k + 1) * block])
-        z_part = z_part + nt_dot(v.xn[k], v.wz[:, k * block : (k + 1) * block])
-    v.xz[me_k] = jnp.concatenate([xs_part * scale, z_part * scale], axis=1).astype(BF16)
-    for k in kv_peers()[::-1]:
-        q = k * nt + me_t
-        send(v.xz.at[me_k], v.xz.at[me_k], m.xz[0].at[k], m.xz[1].at[me_k], q)
-
-    with scope("w_bc"):
-        for k in kv_peers():
-            arrived(v.bc, m.bc, k, k * nt + lead)
-    v.bc[me_k] = bc_row(me_k)[...]
-    summed = sum(v.bc[k] for k in range(nk)) * v.scale[pl.ds(me_k, 1), :]
-    raw = summed[pairs : pairs + 1, :heads] + v.small[0]
-    step = jnp.maximum(raw, 0.0) + jnp.log1p(jnp.exp(-jnp.abs(raw)))
-    decay = jnp.exp(-step * jnp.exp(v.small[1]))
-    step_high, step_low = split_two(step)
-    decay_high, decay_low = split_two(decay)
-    spread = expand(jnp.concatenate([decay_high, decay_low, step_high, step_low], axis=0))
-    decay_row = spread[0:1] + spread[1:2]
-    step_row = spread[2:3] + spread[3:4]
-    bc_new = summed[:pairs].astype(BF16).astype(F32)
-    bconv = silu(hist_bc + bc_new * tap_bc)
-    bmat, cmat = bconv[:groups], bconv[groups:]
-    weight = jnp.sum(bmat * cmat, axis=1, keepdims=True)
-    per_group = nt_dot(cmat.astype(BF16), v.state_b[...])
-    lane = lax.broadcasted_iota(jnp.int32, (groups, flat), 1)
-    low_end = lax.broadcasted_iota(jnp.int32, (groups, flat), 0) * (flat // groups)
-    mine = (lane >= low_end) & (lane < low_end + flat // groups)
-    read = jnp.sum(jnp.where(mine, per_group, 0.0), axis=0, keepdims=True)
-    cross = jnp.sum(jnp.where(mine, weight, 0.0), axis=0, keepdims=True)
-    v.mix[me_k] = jnp.concatenate(
-        [decay_row * read, step_row * cross + v.line[1]], axis=0
-    ).astype(BF16)
-    for k in kv_peers()[::-1]:
-        q = k * nt + me_t
-        send(v.mix.at[me_k], v.mix.at[me_k], m.mix[0].at[k], m.mix[1].at[me_k], q)
-
-    with scope("w_xz"):
-        for k in kv_peers():
-            arrived(v.hist, m.hist, k, k * nt + me_t)
-            arrived(v.xz, m.xz, k, k * nt + me_t)
-    for k in range(nk):
-        at = slice(k * local, (k + 1) * local)
-        past = jnp.concatenate([v.hist[i][:, at] for i in range(nk)], axis=0)
-        v.xconv[:, at] = silu(past + v.xz[k][:, :local].astype(F32) * v.line[0][:, at])
-        v.open[:, at] = silu(v.xz[k][:, local:].astype(F32))
-    loaded("wout")
-    with scope("w_mix"):
-        for k in kv_peers():
-            arrived(v.mix, m.mix, k, k * nt + me_t)
-    pieces = [v.mix[k].astype(F32) for k in range(nk)]
-    read = jnp.concatenate([piece[0:1] for piece in pieces], axis=0)
-    direct = jnp.concatenate([piece[1:2] for piece in pieces], axis=0)
-    mixed = ((read + direct * v.xconv[...]) * v.open[...]).astype(BF16)
-    v.proj[me] = nn_dot(mixed, v.wout[...]).astype(BF16)
-    for q in all_peers()[::-1]:
-        send(v.proj.at[me], v.proj.at[me], m.proj[0].at[q], m.proj[1].at[me], q)
+    squares = jnp.zeros((rows, 1), F32)
+    for x in range(nk):
+        k = flipped(me_k, x)
+        with scope("w_near"):
+            if x:
+                arrived(v.near, m.near, k, k * nt + lead)
+            else:
+                arrived_from_lead(v.near, m.near, k)
+        first = v.near[k].astype(F32)
+        v.first[k] = first
+        left = (first * gain_cut(k, 1)).astype(BF16)
+        squares = squares + jnp.sum(first * first, axis=1, keepdims=True)
+        xs_part = xs_part + nt_dot(left, v.wx[:, columns(k, block)])
+        z_part = z_part + nt_dot(left, v.wz[:, columns(k, block)])
+    scale = lax.rsqrt(squares / dim + EPS)
+    v.scale[...] = jnp.broadcast_to(scale, v.scale.shape)
+    v.xz[me_k, me_t] = jnp.concatenate([xs_part * scale, z_part * scale], axis=1).astype(BF16)
+    for copy in to_leads(v.xz, m.xz):
+        copy.start()
+        sent.append(copy)
+
+    @pl.when(me_t != lead)
+    def _():
+        to_home(v.xz, m.xz).start()
+
+    def proj_sends():
+        for q in all_peers()[::-1]:
+            yield remote(v.proj.at[me_k], v.proj.at[me_k], m.proj[0].at[q], m.proj[1].at[me_k], q)
+
+    @pl.when(me_t == lead)
+    def _():
+        with scope("w_state"):
+            lead_load(2).wait()
+            for t in range(lead):
+                arrived(v.state, m.state, t, me_k * nt + t)
+        for t in range(nt):
+            v.state_b[t] = v.state[t].astype(BF16)
+        with scope("w_bc"):
+            for k in kv_peers():
+                arrived(v.bc, m.bc, k, k * nt + lead)
+        summed = sum(v.bc[k] for k in range(nk)) * v.scale[pl.ds(me_k, 1), :]
+        raw = summed[pairs : pairs + 1, :heads] + v.small[0]
+        step = jnp.maximum(raw, 0.0) + jnp.log1p(jnp.exp(-jnp.abs(raw)))
+        decay = jnp.exp(-step * jnp.exp(v.small[1]))
+        step_high, step_low = split_two(step)
+        decay_high, decay_low = split_two(decay)
+        spread = expand(jnp.concatenate([decay_high, decay_low, step_high, step_low], axis=0))
+        decay_row = spread[0:1] + spread[1:2]
+        step_row = spread[2:3] + spread[3:4]
+        bc_new = summed[:pairs].astype(BF16).astype(F32)
+        bconv = silu(hist_bc + bc_new * tap_bc)
+        bmat, cmat = bconv[:groups], bconv[groups:]
+        weight = jnp.sum(bmat * cmat, axis=1, keepdims=True)
+        lane = lax.broadcasted_iota(jnp.int32, (groups, flat), 1)
+        low_end = lax.broadcasted_iota(jnp.int32, (groups, flat), 0) * (flat // groups)
+        mine = (lane >= low_end) & (lane < low_end + flat // groups)
+        lines = []
+        for t in range(nt):
+            per_group = nt_dot(cmat.astype(BF16), v.state_b[t])
+            read = jnp.sum(jnp.where(mine, per_group, 0.0), axis=0, keepdims=True)
+            lines.append(decay_row * read)
+        cross = jnp.sum(jnp.where(mine, weight, 0.0), axis=0, keepdims=True)
+        lines.append(step_row * cross + v.line[...])
+        v.mix[me_k] = jnp.concatenate(lines, axis=0).astype(BF16)
+
+        def mix_sends():
+            for k in kv_peers()[::-1]:
+                q = k * nt + lead
+                yield remote(v.mix.at[me_k], v.mix.at[me_k], m.mix[0].at[k], m.mix[1].at[me_k], q)
+
+        for copy in mix_sends():
+            copy.start()
+        with scope("w_hist"):
+            for t in range(lead):
+                arrived(v.tap, m.tap, t, me_k * nt + t)
+                arrived_at(v.hist, m.hist, me_k, t)
+            for k in kv_peers():
+                for t in range(nt):
+                    arrived_at(v.hist, m.hist, k, t)
+        with scope("w_wout"):
+            lead_load(3).wait()
+            for t in range(lead):
+                arrived(v.wout, m.wout, t, me_k * nt + t)
+        with scope("w_xz"):
+            for t in range(lead):
+                arrived_at(v.xz, m.xz, me_k, t)
+            for k in kv_peers():
+                for t in range(nt):
+                    arrived_at(v.xz, m.xz, k, t)
+        for t in range(nt):
+            for k in range(nk):
+                at = slice(k * local, (k + 1) * local)
+                past = jnp.concatenate([v.hist[i, t][:, at] for i in range(nk)], axis=0)
+                xs_new = v.xz[k, t][:, :local].astype(F32)
+                v.xconv[t, :, at] = silu(past + xs_new * v.tap[t][:, at])
+                v.open[t, :, at] = silu(v.xz[k, t][:, local:].astype(F32))
+        with scope("w_mix"):
+            for k in kv_peers():
+                arrived(v.mix, m.mix, k, k * nt + lead)
+        pieces = [v.mix[k].astype(F32) for k in range(nk)]
+        direct = jnp.concatenate([piece[nt : nt + 1] for piece in pieces], axis=0)
+        total = jnp.zeros((rows, v.wout.shape[2]), F32)
+        for t in range(nt):
+            read = jnp.concatenate([piece[t : t + 1] for piece in pieces], axis=0)
+            mixed = ((read + direct * v.xconv[t]) * v.open[t]).astype(BF16)
+            total = total + nn_dot(mixed, v.wout[t])
+        v.proj[me_k] = total.astype(BF16)
+        for copy in proj_sends():
+            copy.start()
+        for copy in mix_sends():
+            copy.wait_send()
 
     def arriving_blocks():
         for x in range(nk):
             k = flipped(me_k, x)
             with scope("w_proj"):
-                for d in range(nt):
-                    if x or d:
-                        q = k * nt + lax.rem(me_t + d, nt)
-                        arrived(v.proj, m.proj, q, q)
-            total = sum(v.proj[k * nt + t].astype(F32) for t in range(nt))
-            second = (v.first[k] + total).astype(BF16).astype(F32)
+                if x:
+                    arrived(v.proj, m.proj, k, k * nt + lead)
+                else:
+                    arrived_from_lead(v.proj, m.proj, k)
+            second = (v.first[k] + v.proj[k].astype(F32)).astype(BF16).astype(F32)
             if x == 0:
                 for t in range(nt):
                     v.second[t] = second[:, t * width : (t + 1) * width]
             yield second, gain_cut(k, 2), columns(k, block)
 
     loaded("gate1", "up1")
-    hidden = gated(arriving_blocks(), 1)
+    hidden = gated(arriving_blocks(), 1, nk - 1)
     loaded("down1")
     for x in range(nk)[::-1]:
         k = flipped(me_k, x)
@@ -577,7 +690,20 @@
 
         @pl.when(me_t == lead)
         def _():
+            for copy in first_sends():
+                copy.wait_send()
             for copy in bc_sends():
+                copy.wait_send()
+            for copy in proj_sends():
+                copy.wait_send()
+
+        @pl.when(me_t != lead)
+        def _():
+            slab_home().wait_send()
+            to_home(v.hist, m.hist).wait_send()
+            to_home(v.xz, m.xz).wait_send()
+            tap_home().wait_send()
+            for copy in pushes():
                 copy.wait_send()
 
 
@@ -647,9 +773,9 @@
         wbc=vmem((span * pairs, lanes), BF16),
         wide=vmem((span, pairs * lanes), BF16),
         wdt=vmem((heads, span), BF16),
-        state=vmem((flat, lanes), F32),
-        state_b=vmem((flat, lanes), BF16),
-        wout=vmem((flat, out_cols), BF16),
+        state=vmem((nt, flat, lanes), F32),
+        state_b=vmem((nt, flat, lanes), BF16),
+        wout=vmem((nt, flat, out_cols), BF16),
         small=vmem((3, 1, heads), F32),
         cwx=vmem((taps, half, heads), BF16),
         cwbc=vmem((taps, pairs, lanes), BF16),
@@ -661,28 +787,30 @@
         gain=vmem((n, 3, width), BF16),
         part=vmem((nk, rows, block), BF16),
         slab=vmem((n, rows, block), BF16),
-        full=vmem((n, nk, rows, block), BF16),
+        near=vmem((nk, rows, block), BF16),
+        held=vmem((nk - 1, 2, rows, units), F32),
         first=vmem((nk, rows, block), F32),
-        xn=vmem((nk, rows, block), BF16),
         scale=vmem((rows, lanes), F32),
         bc_b=vmem((nk * (pairs + 8), lanes), F32),
         bc=vmem((nk, pairs + 8, lanes), F32),
-        hist=vmem((nk, 1, flat), F32),
-        line=vmem((2, 1, flat), F32),
-        xz=vmem((nk, rows, 2 * local), BF16),
-        xconv=vmem((rows, flat), F32),
-        open=vmem((rows, flat), F32),
-        mix=vmem((nk, 2, flat), BF16),
-        proj=vmem((n, rows, out_cols), BF16),
+        hist=vmem((nk, nt, 1, flat), F32),
+        tap=vmem((nt, 1, flat), F32),
+        line=vmem((1, flat), F32),
+        xz=vmem((nk, nt, rows, 2 * local), BF16),
+        xconv=vmem((nt, rows, flat), F32),
+        open=vmem((nt, rows, flat), F32),
+        mix=vmem((nk, nt + 1, flat), BF16),
+        proj=vmem((nk, rows, out_cols), BF16),
         second=vmem((nt, rows, width), F32),
         cut_b=vmem((n, rows, width), BF16),
         cut=vmem((n, rows, width), BF16),
     )
     rounds = dict(
-        rows=n, gain=n, slab=n, full=n, bc=n, hist=nk, xz=nk, mix=nk, proj=n, cut=n
+        rows=n, gain=n, slab=n, near=n, bc=n, hist=n, xz=n, mix=nk, state=nt, wout=nt, tap=nt, proj=n, cut=n
     )
     sems = {name: (dma((count,)), dma((count,))) for name, count in rounds.items()}
-    sems["load"] = dma((21,))
+    sems["load"] = dma((17,))
+    sems["lead"] = dma((4,))
 
     def kernel(*refs, **held):
         def body(**flags):

time: 30.8 us -> 28.7 us (0.932)
  Pallas kernels: 30.1 us -> 28 us
    pallas_call x1, Pallas kernels: 30.1 us -> 28 us  [fused_layer(): pl.pallas_call(kernel, out_shape=pltpu.VMEM(resid.shape, resid.dtype), in...]
where the time goes in v3:
time: 28.7 us; the launch traced here: 28.6 us
  Pallas kernels  28 us (98%)
  local copies, waits for them, and re-layouts  0.58 us (2%)
    pallas_call x1, Pallas kernels, fused_layer(): pl.pallas_call(kernel, out_shape=pltpu.VMEM(resid.shape, resid.dtype), in...  28 us
    unnamed x1, local copies, waits for them, and re-layouts  0.58 us

profile of v3, /device:TPU:0, one launch (start us, length us, event | category | flops | bytes accessed | tf_op | source)
XLA Modules:
  0.0 28.6 jit_solution(18330001335090073570)
XLA Ops:
  0.0 28.0 %shard_map.172 = bf16[4,256]{1,0:T(4,128)(2,1)S(1)} custom-call(bf16[4,256]{1,0:T(4,128)(2,1)} %refs_0_.1, bf16[3,256]{1,0:T(4,128)(2,1)} %refs_1_.1, bf16[2,704,2048]{2,1,0:T(8,128)(2,1)} %bitcast.21, bf16[2,704,2048]{2,1,0:T(8,128)(2,1)} %bitcast.22, bf16[2,704,2048]{2,1,0:T(8,128)(2,1)} %refs_4_.1, bf16[512,2048]{1,0:T(8,128)(2,1)} %bitcast.23, ...), custom_call_target="tpu_custom_call" | custom-call | tf_op jit(solution)/shard_map/pallas_call | solution.py:821
  28.0 0.6 %copy.20 = bf16[4,256]{1,0:T(4,128)(2,1)} copy(bf16[4,256]{1,0:T(4,128)(2,1)S(1)} %shard_map.172) | data formatting | bytes 4096

commit v4 on v3

--- a/solution.py
+++ b/solution.py
@@ -351,7 +351,6 @@
     loaded("rows", "gains")
     for q in all_peers()[::-1]:
         send(v.rows.at[me], v.rows.at[me], m.rows[0].at[q], m.rows[1].at[me], q)
-    for q in all_peers()[::-1]:
         send(v.gain.at[me], v.gain.at[me], m.gain[0].at[q], m.gain[1].at[me], q)
 
     home = me_k * nt + lead
@@ -423,15 +422,15 @@
 
     units = v.gate.shape[1]
 
-    def gated(blocks, which, kept):
+    def gated(blocks, kept):
         squares = jnp.zeros((rows, 1), F32)
         g = jnp.zeros((rows, units), F32)
         u = jnp.zeros((rows, units), F32)
         for step, (values, gain, at) in enumerate(blocks):
             squares = squares + jnp.sum(values * values, axis=1, keepdims=True)
             left = (values * gain).astype(BF16)
-            g = g + nt_dot(left, v.gate[which, :, at])
-            u = u + nt_dot(left, v.up[which, :, at])
+            g = g + nn_dot(left, v.gate_t[at, :])
+            u = u + nn_dot(left, v.up_t[at, :])
             if step < kept:
                 v.held[step, 0] = g
                 v.held[step, 1] = u
@@ -443,6 +442,16 @@
         scale = lax.rsqrt(squares / dim + EPS)
         return (silu(g * scale) * (u * scale)).astype(BF16)
 
+    def turn(source, dest):
+        for k in range(dim // 256):
+            at = slice(k * 256, (k + 1) * 256)
+            dest[at, :] = source[:, at].T
+
+    def turn_ffn(which):
+        loaded(f"gate{which}", f"up{which}")
+        turn(v.gate.at[which], v.gate_t)
+        turn(v.up.at[which], v.up_t)
+
     def columns(index, count):
         return pl.ds(pl.multiple_of(index * count, 128), count)
 
@@ -454,8 +463,8 @@
                     arrived(v.gain, m.gain, q, q)
             yield v.rows[q].astype(F32), v.gain[q, 0:1, :].astype(F32), columns(q, width)
 
-    loaded("gate0", "up0")
-    hidden = gated(arriving_rows(), 0, 0)
+    turn_ffn(0)
+    hidden = gated(arriving_rows(), 0)
     loaded("down0")
     for x in range(nk)[::-1]:
         k = flipped(me_k, x)
@@ -506,6 +515,14 @@
                 v.wide[c * deep : (c + 1) * deep, p * 128 : (p + 1) * 128] = piece[
                     p * deep : (p + 1) * deep, :
                 ]
+        with scope("w_state"):
+            lead_load(2).wait()
+            for t in range(lead):
+                arrived(v.state, m.state, t, me_k * nt + t)
+        for t in range(nt):
+            for i in range(flat // 256):
+                at = slice(i * 256, (i + 1) * 256)
+                v.state_b[t, :, at] = v.state[t, at, :].astype(BF16).T
         v.slab[me] = v.part[me_k]
         with scope("w_slab"):
             for q in all_peers():
@@ -537,6 +554,8 @@
             arrived(slots, sems, k, k * nt + lead)
 
     loaded("wx", "wz")
+    turn(v.wx, v.wx_t)
+    turn(v.wz, v.wz_t)
     local = v.wx.shape[0]
     xs_part = jnp.zeros((rows, local), F32)
     z_part = jnp.zeros((rows, local), F32)
@@ -552,8 +571,8 @@
         v.first[k] = first
         left = (first * gain_cut(k, 1)).astype(BF16)
         squares = squares + jnp.sum(first * first, axis=1, keepdims=True)
-        xs_part = xs_part + nt_dot(left, v.wx[:, columns(k, block)])
-        z_part = z_part + nt_dot(left, v.wz[:, columns(k, block)])
+        xs_part = xs_part + nn_dot(left, v.wx_t[columns(k, block), :])
+        z_part = z_part + nn_dot(left, v.wz_t[columns(k, block), :])
     scale = lax.rsqrt(squares / dim + EPS)
     v.scale[...] = jnp.broadcast_to(scale, v.scale.shape)
     v.xz[me_k, me_t] = jnp.concatenate([xs_part * scale, z_part * scale], axis=1).astype(BF16)
@@ -564,6 +583,7 @@
     @pl.when(me_t != lead)
     def _():
         to_home(v.xz, m.xz).start()
+        turn_ffn(1)
 
     def proj_sends():
         for q in all_peers()[::-1]:
@@ -571,12 +591,6 @@
 
     @pl.when(me_t == lead)
     def _():
-        with scope("w_state"):
-            lead_load(2).wait()
-            for t in range(lead):
-                arrived(v.state, m.state, t, me_k * nt + t)
-        for t in range(nt):
-            v.state_b[t] = v.state[t].astype(BF16)
         with scope("w_bc"):
             for k in kv_peers():
                 arrived(v.bc, m.bc, k, k * nt + lead)
@@ -598,7 +612,7 @@
         mine = (lane >= low_end) & (lane < low_end + flat // groups)
         lines = []
         for t in range(nt):
-            per_group = nt_dot(cmat.astype(BF16), v.state_b[t])
+            per_group = nn_dot(cmat.astype(BF16), v.state_b[t])
             read = jnp.sum(jnp.where(mine, per_group, 0.0), axis=0, keepdims=True)
             lines.append(decay_row * read)
         cross = jnp.sum(jnp.where(mine, weight, 0.0), axis=0, keepdims=True)
@@ -612,6 +626,7 @@
 
         for copy in mix_sends():
             copy.start()
+        turn_ffn(1)
         with scope("w_hist"):
             for t in range(lead):
                 arrived(v.tap, m.tap, t, me_k * nt + t)
@@ -666,8 +681,7 @@
                     v.second[t] = second[:, t * width : (t + 1) * width]
             yield second, gain_cut(k, 2), columns(k, block)
 
-    loaded("gate1", "up1")
-    hidden = gated(arriving_blocks(), 1, nk - 1)
+    hidden = gated(arriving_blocks(), nk - 1)
     loaded("down1")
     for x in range(nk)[::-1]:
         k = flipped(me_k, x)
@@ -768,13 +782,17 @@
         gate=vmem((2, units, dim), BF16),
         up=vmem((2, units, dim), BF16),
         down=vmem((2, units, dim), BF16),
+        gate_t=vmem((dim, units), BF16),
+        up_t=vmem((dim, units), BF16),
+        wx_t=vmem((dim, local), BF16),
+        wz_t=vmem((dim, local), BF16),
         wx=vmem((local, dim), BF16),
         wz=vmem((local, dim), BF16),
         wbc=vmem((span * pairs, lanes), BF16),
         wide=vmem((span, pairs * lanes), BF16),
         wdt=vmem((heads, span), BF16),
         state=vmem((nt, flat, lanes), F32),
-        state_b=vmem((nt, flat, lanes), BF16),
+        state_b=vmem((nt, lanes, flat), BF16),
         wout=vmem((nt, flat, out_cols), BF16),
         small=vmem((3, 1, heads), F32),
         cwx=vmem((taps, half, heads), BF16),
@@ -841,6 +859,8 @@
         and nk & (nk - 1) == 0
         and w_bc.shape[0] == nt * width
         and width % 128 == 0
+        and (nk * nt * width) % 256 == 0
+        and (conv_x.shape[2] * conv_x.shape[3]) % 256 == 0
         and w_bc.shape[0] % 128 == 0
         and (w_x.shape[1] * w_x.shape[2]) % 128 == 0
         and half & (half - 1) == 0

time: 28.7 us -> 27.6 us (0.962)
  Pallas kernels: 28 us -> 26.9 us
    pallas_call x1, Pallas kernels: 28 us -> 26.9 us  [fused_layer(): pl.pallas_call(kernel, out_shape=pltpu.VMEM(resid.shape, resid.dtype), in...]
where the time goes in v4:
time: 27.6 us; the launch traced here: 27.5 us
  Pallas kernels  26.9 us (97%)
  local copies, waits for them, and re-layouts  0.58 us (2%)
    pallas_call x1, Pallas kernels, fused_layer(): pl.pallas_call(kernel, out_shape=pltpu.VMEM(resid.shape, resid.dtype), in...  26.9 us
    unnamed x1, local copies, waits for them, and re-layouts  0.58 us

profile of v4, /device:TPU:0, one launch (start us, length us, event | category | flops | bytes accessed | tf_op | source)
XLA Modules:
  0.0 27.5 jit_solution(12227198240564672017)
XLA Ops:
  0.0 26.9 %shard_map.172 = bf16[4,256]{1,0:T(4,128)(2,1)S(1)} custom-call(bf16[4,256]{1,0:T(4,128)(2,1)} %refs_0_.1, bf16[3,256]{1,0:T(4,128)(2,1)} %refs_1_.1, bf16[2,704,2048]{2,1,0:T(8,128)(2,1)} %bitcast.21, bf16[2,704,2048]{2,1,0:T(8,128)(2,1)} %bitcast.22, bf16[2,704,2048]{2,1,0:T(8,128)(2,1)} %refs_4_.1, bf16[512,2048]{1,0:T(8,128)(2,1)} %bitcast.23, ...), custom_call_target="tpu_custom_call" | custom-call | tf_op jit(solution)/shard_map/pallas_call | solution.py:839
  26.9 0.6 %copy.20 = bf16[4,256]{1,0:T(4,128)(2,1)} copy(bf16[4,256]{1,0:T(4,128)(2,1)S(1)} %shard_map.172) | data formatting | bytes 4096

commit v5 on v4

--- a/solution.py
+++ b/solution.py
@@ -270,6 +270,10 @@
         order = [(x, d) for x in range(nk) for d in range(nt)][1:]
         return [flipped(me_k, x) * nt + lax.rem(me_t + d, nt) for x, d in order]
 
+    def far_first():
+        far = [flipped(me_k, x) * nt + t for x in range(1, nk)[::-1] for t in range(nt)]
+        return far + [me_k * nt + lax.rem(me_t + d, nt) for d in range(1, nt)]
+
     def kv_peers():
         return [flipped(me_k, x) for x in range(1, nk)]
 
@@ -288,7 +292,7 @@
     load("rows", resid, v.rows.at[me])
     load("gains", gains, v.gain.at[me])
     barrier = pltpu.get_barrier_semaphore()
-    for q in all_peers()[::-1]:
+    for q in far_first():
         pl.semaphore_signal(barrier, inc=1, device_id=target(q), device_id_type=MESH)
     load("bias", dt_bias, v.small.at[0])
     load("alog", a_log, v.small.at[1])
@@ -349,7 +353,7 @@
         remote(slots.at[slot], slots.at[slot], sems[0].at[slot], sems[1].at[slot], index).wait_recv()
 
     loaded("rows", "gains")
-    for q in all_peers()[::-1]:
+    for q in far_first():
         send(v.rows.at[me], v.rows.at[me], m.rows[0].at[q], m.rows[1].at[me], q)
         send(v.gain.at[me], v.gain.at[me], m.gain[0].at[q], m.gain[1].at[me], q)
 
@@ -392,8 +396,6 @@
         jnp.where(own, expand(high) + expand(low), 0.0), axis=0, keepdims=True
     )
     v.tap[me_t] = jnp.sum(jnp.where(own, expand(v.cwx[taps]), 0.0), axis=0, keepdims=True)
-    skip_high, skip_low = split_two(v.small[2])
-    v.line[...] = expand(skip_high) + expand(skip_low)
 
     def to_leads(ref, sems):
         for k in kv_peers()[::-1]:
@@ -455,8 +457,13 @@
     def columns(index, count):
         return pl.ds(pl.multiple_of(index * count, 128), count)
 
+    def by_arrival():
+        order = [lead - d for d in range(nt)]
+        near = [me_k * nt + lax.rem(me_t + d, nt) for d in range(1, nt)]
+        return near + [flipped(me_k, x) * nt + t for x in range(1, nk) for t in order]
+
     def arriving_rows():
-        for q in [me] + all_peers():
+        for q in [me] + by_arrival():
             if q is not me:
                 with scope("w_rows"):
                     arrived(v.rows, m.rows, q, q)
@@ -495,7 +502,7 @@
         return v.bc_b.at[pl.ds(pl.multiple_of(k * tall, 8), tall), :]
 
     def first_sends():
-        for q in all_peers()[::-1]:
+        for q in far_first():
             yield remote(v.near.at[me_k], v.near.at[me_k], m.near[0].at[q], m.near[1].at[me_k], q)
 
     def bc_sends():
@@ -586,7 +593,7 @@
         turn_ffn(1)
 
     def proj_sends():
-        for q in all_peers()[::-1]:
+        for q in far_first():
             yield remote(v.proj.at[me_k], v.proj.at[me_k], m.proj[0].at[q], m.proj[1].at[me_k], q)
 
     @pl.when(me_t == lead)
@@ -598,15 +605,28 @@
         raw = summed[pairs : pairs + 1, :heads] + v.small[0]
         step = jnp.maximum(raw, 0.0) + jnp.log1p(jnp.exp(-jnp.abs(raw)))
         decay = jnp.exp(-step * jnp.exp(v.small[1]))
-        step_high, step_low = split_two(step)
-        decay_high, decay_low = split_two(decay)
-        spread = expand(jnp.concatenate([decay_high, decay_low, step_high, step_low], axis=0))
-        decay_row = spread[0:1] + spread[1:2]
-        step_row = spread[2:3] + spread[3:4]
         bc_new = summed[:pairs].astype(BF16).astype(F32)
         bconv = silu(hist_bc + bc_new * tap_bc)
         bmat, cmat = bconv[:groups], bconv[groups:]
         weight = jnp.sum(bmat * cmat, axis=1, keepdims=True)
+        lane = lax.broadcasted_iota(jnp.int32, (groups, heads), 1)
+        low_end = lax.broadcasted_iota(jnp.int32, (groups, heads), 0) * (heads // groups)
+        mine = (lane >= low_end) & (lane < low_end + heads // groups)
+        cross = jnp.sum(jnp.where(mine, weight, 0.0), axis=0, keepdims=True)
+        v.coef[me_k] = step * cross + v.small[2]
+
+        def coef_sends():
+            for k in kv_peers()[::-1]:
+                q = k * nt + lead
+                yield remote(
+                    v.coef.at[me_k], v.coef.at[me_k], m.coef[0].at[k], m.coef[1].at[me_k], q
+                )
+
+        for copy in coef_sends():
+            copy.start()
+        decay_high, decay_low = split_two(decay)
+        spread = expand(jnp.concatenate([decay_high, decay_low], axis=0))
+        decay_row = spread[0:1] + spread[1:2]
         lane = lax.broadcasted_iota(jnp.int32, (groups, flat), 1)
         low_end = lax.broadcasted_iota(jnp.int32, (groups, flat), 0) * (flat // groups)
         mine = (lane >= low_end) & (lane < low_end + flat // groups)
@@ -615,8 +635,6 @@
             per_group = nn_dot(cmat.astype(BF16), v.state_b[t])
             read = jnp.sum(jnp.where(mine, per_group, 0.0), axis=0, keepdims=True)
             lines.append(decay_row * read)
-        cross = jnp.sum(jnp.where(mine, weight, 0.0), axis=0, keepdims=True)
-        lines.append(step_row * cross + v.line[...])
         v.mix[me_k] = jnp.concatenate(lines, axis=0).astype(BF16)
 
         def mix_sends():
@@ -638,33 +656,41 @@
             lead_load(3).wait()
             for t in range(lead):
                 arrived(v.wout, m.wout, t, me_k * nt + t)
-        with scope("w_xz"):
-            for t in range(lead):
-                arrived_at(v.xz, m.xz, me_k, t)
+        for t in range(nt):
+            v.past[t] = jnp.concatenate([v.hist[i, t] for i in range(nk)], axis=0)
+        with scope("w_coef"):
             for k in kv_peers():
-                for t in range(nt):
-                    arrived_at(v.xz, m.xz, k, t)
-        for t in range(nt):
-            for k in range(nk):
-                at = slice(k * local, (k + 1) * local)
-                past = jnp.concatenate([v.hist[i, t][:, at] for i in range(nk)], axis=0)
-                xs_new = v.xz[k, t][:, :local].astype(F32)
-                v.xconv[t, :, at] = silu(past + xs_new * v.tap[t][:, at])
-                v.open[t, :, at] = silu(v.xz[k, t][:, local:].astype(F32))
+                arrived(v.coef, m.coef, k, k * nt + lead)
+        high, low = split_two(jnp.concatenate([v.coef[i] for i in range(nk)], axis=0))
+        spread = expand(jnp.concatenate([high, low], axis=0))
+        v.direct[...] = spread[:nk] + spread[nk:]
         with scope("w_mix"):
             for k in kv_peers():
                 arrived(v.mix, m.mix, k, k * nt + lead)
-        pieces = [v.mix[k].astype(F32) for k in range(nk)]
-        direct = jnp.concatenate([piece[nt : nt + 1] for piece in pieces], axis=0)
         total = jnp.zeros((rows, v.wout.shape[2]), F32)
-        for t in range(nt):
-            read = jnp.concatenate([piece[t : t + 1] for piece in pieces], axis=0)
-            mixed = ((read + direct * v.xconv[t]) * v.open[t]).astype(BF16)
-            total = total + nn_dot(mixed, v.wout[t])
+        for x in range(nk):
+            k = flipped(me_k, x)
+            at = columns(k, local)
+            with scope("w_xz"):
+                for t in range(nt)[::-1]:
+                    if x or t != lead:
+                        arrived_at(v.xz, m.xz, k, t)
+            direct = v.direct[:, at]
+            for t in range(nt):
+                read = jnp.concatenate(
+                    [v.mix[i, t : t + 1, at].astype(F32) for i in range(nk)], axis=0
+                )
+                xs_new = v.xz[k, t, :, :local].astype(F32)
+                xconv = silu(v.past[t, :, at] + xs_new * v.tap[t, :, at])
+                opened = silu(v.xz[k, t, :, local:].astype(F32))
+                mixed = ((read + direct * xconv) * opened).astype(BF16)
+                total = total + nn_dot(mixed, v.wout[t, at, :])
         v.proj[me_k] = total.astype(BF16)
         for copy in proj_sends():
             copy.start()
         for copy in mix_sends():
+            copy.wait_send()
+        for copy in coef_sends():
             copy.wait_send()
 
     def arriving_blocks():
@@ -688,18 +714,13 @@
         piece = nn_dot(hidden, v.down[1, :, columns(k, block)])
         for t in range(nt):
             v.cut_b[k * nt + t] = piece[:, t * width : (t + 1) * width].astype(BF16)
-        for d in range(nt)[::-1]:
+        for d in range(nt):
             if x or d:
-                q = k * nt + lax.rem(me_t + d, nt)
+                q = k * nt + (d if x else lax.rem(me_t + d, nt))
                 send(v.cut_b.at[q], v.cut.at[me], m.cut[0].at[q], m.cut[1].at[me], q)
     v.cut[me] = v.cut_b[me]
-    with scope("w_cut"):
-        for q in all_peers():
-            arrived(v.cut, m.cut, q, q)
-    total = sum(v.cut[q].astype(F32) for q in range(n))
-    out[...] = (v.second[me_t] + 0.5 * total).astype(BF16)
     with scope("w_sent"):
-        for copy in sent:
+        for copy in sent[:-(n - 1)]:
             copy.wait_send()
 
         @pl.when(me_t == lead)
@@ -719,6 +740,13 @@
             tap_home().wait_send()
             for copy in pushes():
                 copy.wait_send()
+    with scope("w_cut"):
+        for q in all_peers():
+            arrived(v.cut, m.cut, q, q)
+    total = sum(v.cut[q].astype(F32) for q in range(n))
+    out[...] = (v.second[me_t] + 0.5 * total).astype(BF16)
+    for copy in sent[-(n - 1) :]:
+        copy.wait_send()
 
 
 def fused_layer(
@@ -813,18 +841,18 @@
         bc=vmem((nk, pairs + 8, lanes), F32),
         hist=vmem((nk, nt, 1, flat), F32),
         tap=vmem((nt, 1, flat), F32),
-        line=vmem((1, flat), F32),
         xz=vmem((nk, nt, rows, 2 * local), BF16),
-        xconv=vmem((nt, rows, flat), F32),
-        open=vmem((nt, rows, flat), F32),
-        mix=vmem((nk, nt + 1, flat), BF16),
+        past=vmem((nt, rows, flat), F32),
+        coef=vmem((nk, 1, heads), F32),
+        direct=vmem((nk, flat), F32),
+        mix=vmem((nk, nt, flat), BF16),
         proj=vmem((nk, rows, out_cols), BF16),
         second=vmem((nt, rows, width), F32),
         cut_b=vmem((n, rows, width), BF16),
         cut=vmem((n, rows, width), BF16),
     )
     rounds = dict(
-        rows=n, gain=n, slab=n, near=n, bc=n, hist=n, xz=n, mix=nk, state=nt, wout=nt, tap=nt, proj=n, cut=n
+        rows=n, gain=n, slab=n, near=n, bc=n, hist=n, xz=n, mix=nk, coef=nk, state=nt, wout=nt, tap=nt, proj=n, cut=n
     )
     sems = {name: (dma((count,)), dma((count,))) for name, count in rounds.items()}
     sems["load"] = dma((17,))

time: 27.6 us -> 26.9 us (0.975)
  Pallas kernels: 26.9 us -> 26.2 us
    pallas_call x1, Pallas kernels: 26.9 us -> 26.2 us  [fused_layer(): pl.pallas_call(kernel, out_shape=pltpu.VMEM(resid.shape, resid.dtype), in...]
where the time goes in v5:
time: 26.9 us; the launch traced here: 26.8 us
  Pallas kernels  26.2 us (97%)
  local copies, waits for them, and re-layouts  0.58 us (2%)
    pallas_call x1, Pallas kernels, fused_layer(): pl.pallas_call(kernel, out_shape=pltpu.VMEM(resid.shape, resid.dtype), in...  26.2 us
    unnamed x1, local copies, waits for them, and re-layouts  0.58 us

profile of v5, /device:TPU:0, one launch (start us, length us, event | category | flops | bytes accessed | tf_op | source)
XLA Modules:
  0.0 26.8 jit_solution(5033105714581683620)
XLA Ops:
  0.0 26.2 %shard_map.172 = bf16[4,256]{1,0:T(4,128)(2,1)S(1)} custom-call(bf16[4,256]{1,0:T(4,128)(2,1)} %refs_0_.1, bf16[3,256]{1,0:T(4,128)(2,1)} %refs_1_.1, bf16[2,704,2048]{2,1,0:T(8,128)(2,1)} %bitcast.21, bf16[2,704,2048]{2,1,0:T(8,128)(2,1)} %bitcast.22, bf16[2,704,2048]{2,1,0:T(8,128)(2,1)} %refs_4_.1, bf16[512,2048]{1,0:T(8,128)(2,1)} %bitcast.23, ...), custom_call_target="tpu_custom_call" | custom-call | tf_op jit(solution)/shard_map/pallas_call | solution.py:867
  26.2 0.6 %copy.20 = bf16[4,256]{1,0:T(4,128)(2,1)} copy(bf16[4,256]{1,0:T(4,128)(2,1)S(1)} %shard_map.172) | data formatting | bytes 4096

commit v6 on v5

--- a/solution.py
+++ b/solution.py
@@ -450,8 +450,9 @@
             dest[at, :] = source[:, at].T
 
     def turn_ffn(which):
-        loaded(f"gate{which}", f"up{which}")
+        loaded(f"gate{which}")
         turn(v.gate.at[which], v.gate_t)
+        loaded(f"up{which}")
         turn(v.up.at[which], v.up_t)
 
     def columns(index, count):
@@ -502,7 +503,8 @@
         return v.bc_b.at[pl.ds(pl.multiple_of(k * tall, 8), tall), :]
 
     def first_sends():
-        for q in far_first():
+        order = far_first()
+        for q in order[1:-1:nt] + order[::nt]:
             yield remote(v.near.at[me_k], v.near.at[me_k], m.near[0].at[q], m.near[1].at[me_k], q)
 
     def bc_sends():

time: 26.9 us -> 26.9 us (level)
  no operation moved by 1% of the time
where the time goes in v6:
time: 26.9 us; the launch traced here: 26.7 us
  Pallas kernels  26.1 us (97%)
  local copies, waits for them, and re-layouts  0.58 us (2%)
    pallas_call x1, Pallas kernels, fused_layer(): pl.pallas_call(kernel, out_shape=pltpu.VMEM(resid.shape, resid.dtype), in...  26.1 us
    unnamed x1, local copies, waits for them, and re-layouts  0.58 us

profile of v6, /device:TPU:0, one launch (start us, length us, event | category | flops | bytes accessed | tf_op | source)
XLA Modules:
  0.0 26.7 jit_solution(10197966223806187415)
XLA Ops:
  0.0 26.1 %shard_map.172 = bf16[4,256]{1,0:T(4,128)(2,1)S(1)} custom-call(bf16[4,256]{1,0:T(4,128)(2,1)} %refs_0_.1, bf16[3,256]{1,0:T(4,128)(2,1)} %refs_1_.1, bf16[2,704,2048]{2,1,0:T(8,128)(2,1)} %bitcast.21, bf16[2,704,2048]{2,1,0:T(8,128)(2,1)} %bitcast.22, bf16[2,704,2048]{2,1,0:T(8,128)(2,1)} %refs_4_.1, bf16[512,2048]{1,0:T(8,128)(2,1)} %bitcast.23, ...), custom_call_target="tpu_custom_call" | custom-call | tf_op jit(solution)/shard_map/pallas_call | solution.py:869
  26.1 0.6 %copy.20 = bf16[4,256]{1,0:T(4,128)(2,1)} copy(bf16[4,256]{1,0:T(4,128)(2,1)S(1)} %shard_map.172) | data formatting | bytes 4096

commit v7 on v6

--- a/solution.py
+++ b/solution.py
@@ -474,12 +474,15 @@
     turn_ffn(0)
     hidden = gated(arriving_rows(), 0)
     loaded("down0")
-    for x in range(nk)[::-1]:
-        k = flipped(me_k, x)
-        v.part[k] = nn_dot(hidden, v.down[0, :, columns(k, block)]).astype(BF16)
-        q = k * nt + lead
-        if x:
-            send(v.part.at[k], v.slab.at[me], m.slab[0].at[q], m.slab[1].at[me], q)
+    for far in ((nk - 1,), tuple(range(nk - 1))[::-1]):
+        pieces = {x: nn_dot(hidden, v.down[0, :, columns(flipped(me_k, x), block)]) for x in far}
+        for x in far:
+            v.part[flipped(me_k, x)] = pieces[x].astype(BF16)
+        for x in far:
+            k = flipped(me_k, x)
+            q = k * nt + lead
+            if x:
+                send(v.part.at[k], v.slab.at[me], m.slab[0].at[q], m.slab[1].at[me], q)
 
     def slab_home():
         q = me_k * nt + lead
@@ -711,15 +714,18 @@
 
     hidden = gated(arriving_blocks(), nk - 1)
     loaded("down1")
-    for x in range(nk)[::-1]:
-        k = flipped(me_k, x)
-        piece = nn_dot(hidden, v.down[1, :, columns(k, block)])
-        for t in range(nt):
-            v.cut_b[k * nt + t] = piece[:, t * width : (t + 1) * width].astype(BF16)
-        for d in range(nt):
-            if x or d:
-                q = k * nt + (d if x else lax.rem(me_t + d, nt))
-                send(v.cut_b.at[q], v.cut.at[me], m.cut[0].at[q], m.cut[1].at[me], q)
+    for far in ((nk - 1,), tuple(range(nk - 1))[::-1]):
+        pieces = {x: nn_dot(hidden, v.down[1, :, columns(flipped(me_k, x), block)]) for x in far}
+        for x in far:
+            k = flipped(me_k, x)
+            for t in range(nt):
+                v.cut_b[k * nt + t] = pieces[x][:, t * width : (t + 1) * width].astype(BF16)
+        for x in far:
+            k = flipped(me_k, x)
+            for d in range(nt):
+                if x or d:
+                    q = k * nt + (d if x else lax.rem(me_t + d, nt))
+                    send(v.cut_b.at[q], v.cut.at[me], m.cut[0].at[q], m.cut[1].at[me], q)
     v.cut[me] = v.cut_b[me]
     with scope("w_sent"):
         for copy in sent[:-(n - 1)]:

time: 26.9 us -> 26.9 us (level)
  no operation moved by 1% of the time
where the time goes in v7:
time: 26.9 us; the launch traced here: 26.7 us
  Pallas kernels  26.1 us (97%)
  local copies, waits for them, and re-layouts  0.58 us (2%)
    pallas_call x1, Pallas kernels, fused_layer(): pl.pallas_call(kernel, out_shape=pltpu.VMEM(resid.shape, resid.dtype), in...  26.1 us
    unnamed x1, local copies, waits for them, and re-layouts  0.58 us

profile of v7, /device:TPU:0, one launch (start us, length us, event | category | flops | bytes accessed | tf_op | source)
XLA Modules:
  0.0 26.7 jit_solution(2643230692222981145)
XLA Ops:
  0.0 26.1 %shard_map.172 = bf16[4,256]{1,0:T(4,128)(2,1)S(1)} custom-call(bf16[4,256]{1,0:T(4,128)(2,1)} %refs_0_.1, bf16[3,256]{1,0:T(4,128)(2,1)} %refs_1_.1, bf16[2,704,2048]{2,1,0:T(8,128)(2,1)} %bitcast.21, bf16[2,704,2048]{2,1,0:T(8,128)(2,1)} %bitcast.22, bf16[2,704,2048]{2,1,0:T(8,128)(2,1)} %refs_4_.1, bf16[512,2048]{1,0:T(8,128)(2,1)} %bitcast.23, ...), custom_call_target="tpu_custom_call" | custom-call | tf_op jit(solution)/shard_map/pallas_call | solution.py:875
  26.1 0.6 %copy.20 = bf16[4,256]{1,0:T(4,128)(2,1)} copy(bf16[4,256]{1,0:T(4,128)(2,1)S(1)} %shard_map.172) | data formatting | bytes 4096
